TPU v7x, 256 devices: a whole 4x4x8 slice. The times are simulated.
256 devices in a mesh: sp: 32 (over z, y), fs: 4 (over x), tp: 2 (over core).
Axes of the slice: x: 4, y: 4, z: 8, core: 2. Of those that a mesh axis runs over, the one named last changes fastest.
Arguments:
- tokens: bfloat16 [4, 24576, 2048], P('fs', 'sp', 'tp'), may hold values from -6 to 6
- in_gain: float32 [2048], replicated, may hold values from 0.1 to 1.9
- ret_query: bfloat16 [2048, 768], P(None, 'tp'), may hold values from -0.125 to 0.125
- ret_key: bfloat16 [2048, 768], P(None, 'tp'), may hold values from -0.125 to 0.125
- ret_value: bfloat16 [2048, 768], P(None, 'tp'), may hold values from -0.125 to 0.125
- att_query: bfloat16 [2048, 768], P(None, 'tp'), may hold values from -8 to 8
- att_key: bfloat16 [2048, 256], P(None, 'tp'), may hold values from -8 to 8
- att_value: bfloat16 [2048, 256], P(None, 'tp'), may hold values from -0.125 to 0.125
- log_decay: float32 [4, 12, 24576], P('fs', 'tp', 'sp'), may hold values from -1.5 to 0
- ret_gain: float32 [768], P('tp'), may hold values from 0.1 to 1.9
- sink_logit: float32 [12], P('tp'), may hold values from 1 to 5
- retentive_exit_matrix: bfloat16 [768, 2048], P('tp'), may hold values from -0.15625 to 0.15625
- out_att: bfloat16 [768, 2048], P('tp'), may hold values from -0.875 to 0.875
Outputs:
- mixed: bfloat16 [4, 24576, 2048], P('fs', ('sp', 'tp'))
All inputs are finite; a program needn't handle non-finite values.
Results may differ from a plain program's by a relative error of at most 0.0085.
Values may be sent and summed in bfloat16 or wider, within the bound.
A program may use at most 128 MiB of HBM per device.

v0:
```python
import jax
import jax.numpy as jnp
from jax import lax
from jax.sharding import Mesh
from jax.sharding import PartitionSpec as P

HEAD_DIM = 64
WINDOW = 128
SP = ("sp_0", "sp_1")
SP_TP = ("sp_0", "sp_1", "tp")


EPS = 1e-06


def nothing_yet(value, identity):
    return jax.tree.map(
        lambda part, zero: jnp.zeros_like(part) + jnp.asarray(zero, part.dtype), value, identity
    )


def entering(value, axes, combine, identity):
    before = start = nothing_yet(value, identity)
    total = value
    for axis in reversed(axes):
        peers, position = (lax.axis_size(axis), lax.axis_index(axis))
        pieces = jax.tree.map(
            lambda part, kind: lax.all_gather(part.astype(kind), axis),
            total,
            (jnp.bfloat16, jnp.bfloat16),
        )
        inside, total = (start, start)
        for k in range(peers):
            passed = k < position
            total = combine(
                total, jax.tree.map(lambda part, own: part[k].astype(own.dtype), pieces, value)
            )
            inside = jax.tree.map(lambda new, old: jnp.where(passed, new, old), total, inside)
        before = combine(inside, before)
    return before


def passed_along(value, axis, by):
    peers = lax.axis_size(axis)
    pairs = [(i, i + by) for i in range(peers) if 0 <= i + by < peers]
    return lax.ppermute(value, axis, pairs)


def attend_window(query_rows, key_ext, value_ext, first_position, sinks):
    length = query_rows.shape[0]
    blocks = length // WINDOW
    heads_kv = key_ext.shape[1] // HEAD_DIM
    heads = query_rows.shape[1] // HEAD_DIM
    group = heads // heads_kv
    shaped_q = query_rows.reshape(blocks, WINDOW, heads_kv, group, HEAD_DIM)
    key_block_list = key_ext.reshape(blocks + 1, WINDOW, heads_kv, HEAD_DIM)
    value_blocks = value_ext.reshape(blocks + 1, WINDOW, heads_kv, HEAD_DIM)
    key_band = jnp.concatenate([key_block_list[:-1], key_block_list[1:]], axis=1)
    value_band = jnp.concatenate([value_blocks[:-1], value_blocks[1:]], axis=1)
    scores = jnp.einsum(
        "nqhgd,nkhd->hgnqk", shaped_q, key_band, preferred_element_type=jnp.float32
    ) * HEAD_DIM ** (-0.5)
    distance = WINDOW + jnp.arange(WINDOW)[:, None] - jnp.arange(2 * WINDOW)[None, :]
    key_position = (
        first_position
        - WINDOW
        + jnp.arange(blocks)[:, None] * WINDOW
        + jnp.arange(2 * WINDOW)[None, :]
    )
    allowed = ((distance >= 0) & (distance < WINDOW))[None] & (key_position >= 0)[:, None, :]
    scores = jnp.where(allowed, scores, -jnp.inf)
    sink_part = sinks.reshape(heads_kv, group, 1, 1, 1)
    greatest_level = jnp.maximum(jnp.max(scores, axis=-1, keepdims=True), sink_part)
    raised = jnp.exp(scores - greatest_level)
    totals = jnp.sum(raised, axis=-1, keepdims=True) + jnp.exp(sink_part - greatest_level)
    weights = (raised / totals).astype(jnp.bfloat16)
    outputs = jnp.einsum(
        "hgnqk,nkhd->nqhgd", weights, value_band, preferred_element_type=jnp.float32
    )
    return outputs.reshape(length, heads * HEAD_DIM).astype(jnp.bfloat16)


def shards(
    tokens,
    in_gain,
    ret_query,
    ret_key,
    ret_value,
    att_query,
    att_key,
    att_value,
    log_decay,
    ret_gain,
    sink_logit,
    retentive_exit_matrix,
    out_att,
):
    rows_here = tokens.shape[1]
    model_width = in_gain.shape[0]
    projections = (ret_query, ret_key, ret_value, att_query, att_key, att_value)
    wide = lax.all_gather(tokens, "tp", axis=2, tiled=True)[0].astype(jnp.float32)
    scaled = (wide * in_gain).astype(jnp.bfloat16)
    sums = tuple(
        (jnp.dot(scaled, weight, preferred_element_type=jnp.float32) for weight in projections)
    )
    sums, squares = (sums, jnp.sum(wide * wide, axis=1, keepdims=True))
    inverse = lax.rsqrt(squares / model_width + EPS)
    ret_q, ret_k, ret_v, att_q, att_k, att_v = [
        (total * inverse).astype(jnp.bfloat16) for total in sums
    ]
    rates = log_decay[0]
    heads = rates.shape[0]
    fading_multiplier = HEAD_DIM ** (-0.5)
    cumulative = jnp.cumsum(rates, axis=1)
    later = jnp.arange(rows_here)[:, None] >= jnp.arange(rows_here)[None, :]
    decay = jnp.exp(
        jnp.where(later[None], cumulative[:, :, None] - cumulative[:, None, :], -jnp.inf)
    )
    shaped_q = ret_q.reshape(rows_here, heads, HEAD_DIM)
    shaped_k = ret_k.reshape(rows_here, heads, HEAD_DIM)
    shaped_v = ret_v.reshape(rows_here, heads, HEAD_DIM)
    weights = (
        jnp.einsum("thd,shd->hts", shaped_q, shaped_k, preferred_element_type=jnp.float32)
        * fading_multiplier
        * decay
    ).astype(jnp.bfloat16)
    inner = jnp.einsum("hts,shd->thd", weights, shaped_v, preferred_element_type=jnp.float32)
    keyed = (
        shaped_k.astype(jnp.float32)
        * (jnp.exp(cumulative[:, -1:] - cumulative) * fading_multiplier).T[:, :, None]
    )
    own_state = jnp.einsum("shd,she->hde", keyed, shaped_v.astype(jnp.float32))
    total_rate = jnp.exp(cumulative[:, -1])
    tail_keys = att_k[rows_here - WINDOW :]
    trailing_values = att_v[rows_here - WINDOW :]

    def combine(earlier, later_part):
        return (
            earlier[0] * later_part[0],
            later_part[0][:, None, None] * earlier[1] + later_part[1],
        )

    identity = (jnp.ones_like(total_rate), jnp.zeros_like(own_state))
    prefix = entering((total_rate, own_state), SP, combine, identity)
    incoming = prefix[1]
    before_keys, before_values = passed_along((tail_keys, trailing_values), SP, 1)
    carried = jnp.einsum("thd,hde->the", shaped_q.astype(jnp.float32), incoming)
    retained = inner + carried * jnp.exp(cumulative).T[:, :, None]
    normed = retained * lax.rsqrt(jnp.mean(retained * retained, axis=-1, keepdims=True) + EPS)
    ret_out = (normed.reshape(rows_here, heads * HEAD_DIM) * ret_gain).astype(jnp.bfloat16)
    first_position = lax.axis_index(SP) * rows_here
    key_ext = jnp.concatenate([before_keys, att_k], axis=0)
    value_ext = jnp.concatenate([before_values, att_v], axis=0)
    att_out = attend_window(att_q, key_ext, value_ext, first_position, sink_logit)
    ret_rows, att_rows = (
        lax.all_to_all(ret_out, "tp", split_axis=0, concat_axis=1, tiled=True),
        lax.all_to_all(att_out, "tp", split_axis=0, concat_axis=1, tiled=True),
    )
    summed = jnp.dot(
        ret_rows,
        lax.all_gather(retentive_exit_matrix, "tp", axis=0, tiled=True),
        preferred_element_type=jnp.float32,
    ) + jnp.dot(
        att_rows,
        lax.all_gather(out_att, "tp", axis=0, tiled=True),
        preferred_element_type=jnp.float32,
    )
    return summed.astype(jnp.bfloat16)[None]


def solution(mesh):
    finer = Mesh(
        mesh.devices.reshape(8, 4, mesh.shape["fs"], mesh.shape["tp"]), ("sp_0", "sp_1", "fs", "tp")
    )
    placed = (
        P("fs", SP, "tp"),
        P(),
        P(None, "tp"),
        P(None, "tp"),
        P(None, "tp"),
        P(None, "tp"),
        P(None, "tp"),
        P(None, "tp"),
        P("fs", "tp", SP),
        P("tp"),
        P("tp"),
        P("tp", None),
        P("tp", None),
    )
    return jax.shard_map(
        shards, mesh=finer, in_specs=placed, out_specs=P("fs", SP_TP, None), check_vma=False
    )
```

profile of v0, /device:TPU:1, one launch (start us, length us, event | category | flops | bytes accessed | tf_op | source)
XLA Modules:
  0.0 154.9 jit_solution(6653414985704127951)
XLA Ops:
  8.9 1.7 %reduce-window.6 = f32[6,6,128]{2,1,0:T(8,128)S(1)} reduce-window(f32[6,6,128]{2,1,0:T(8,128)S(1)} %reshape.321, f32[]{:T(128)} %constant.21.clone.1), window={size=1x1x128 pad=0_0x0_0x127_0}, to_apply=%region_1.0 | reduce-window | flops 585216 | bytes 36868 | tf_op jit(solution)/shard_map/reduce-window
  13.7 9.5 %all-reduce = bf16[24]{0:T(256)(128)(2,1)S(1)} all-reduce(bf16[24]{0:T(256)(128)(2,1)S(1)} %dynamic-update-slice), channel_id=2, replica_groups=mesh['sp_0'=8,'sp_1'=4,'fs'=4,'tp'=2] {'sp_1'}, use_global_device_ids=true, to_apply=%add | all-reduce | flops 24 | bytes 96
  23.3 15.4 %all-gather.2 = bf16[8,1,6]{2,1,0:T(2,128)(2,1)S(1)} all-gather(bf16[1,1,6]{2,1,0:T(2,128)(2,1)S(1)} %fusion.133), channel_id=1, replica_groups=mesh['sp_0'=8,'sp_1'=4,'fs'=4,'tp'=2] {'sp_0'}, dimensions={0}, use_global_device_ids=true | all-gather | bytes 108 | tf_op jit(solution)/shard_map/all_gather | solution.py:28
  39.4 2.7 %fusion.1 = f32[768]{0:T(1024)S(1)} fusion(bf16[1,768,2048]{2,1,0:T(8,128)(2,1)} %all-gather.7.cloned.1.call-done), kind=kLoop, calls=%fused_computation.4 | loop fusion | flops 4717824 | bytes 3148800 | tf_op jit(solution)/shard_map/reduce_sum | solution.py:106
  43.3 1.4 collective-permute-start.1
  44.7 1.4 fusion.13
  46.2 1.4 fusion.11
  47.9 9.8 %all-gather.1 = bf16[24,64,64]{2,1,0:T(8,128)(2,1)S(1)} all-gather(bf16[6,64,64]{2,1,0:T(8,128)(2,1)S(1)} %fusion.45), channel_id=3, replica_groups=mesh['sp_0'=8,'sp_1'=4,'fs'=4,'tp'=2] {'sp_1'}, dimensions={0}, use_global_device_ids=true | all-gather | bytes 245760 | tf_op jit(solution)/shard_map/all_gather | solution.py:28
  57.9 19.8 %all_gather.32 = bf16[8,6,64,64]{3,2,1,0:T(8,128)(2,1)S(1)} all-gather(bf16[1,6,64,64]{3,2,1,0:T(8,128)(2,1)S(1)} %fusion.69), channel_id=1, replica_groups=mesh['sp_0'=8,'sp_1'=4,'fs'=4,'tp'=2] {'sp_0'}, dimensions={0}, use_global_device_ids=true | all-gather | bytes 442368 | tf_op jit(solution)/shard_map/all_gather | solution.py:28
  77.6 2.3 %fusion.12 = bf16[768,384]{0,1:T(8,128)(2,1)} fusion(bf16[2048,384]{1,0:T(8,128)(2,1)S(1)} %copy-done.6, bf16[1,768,2048]{2,1,0:T(8,128)(2,1)S(1)} %copy-done.1, f32[2048]{0:T(1024)S(1)} %copy-done.10, f32[768]{0:T(1024)S(1)} %add_rsqrt_fusion.1), kind=kOutput, calls=%fused_computation.25 | convolution fusion | flops 1213267968 | bytes 5319680 | tf_op jit(solution)/shard_map/dot_general | solution.py:104
  79.9 8.6 %fusion.8 = f32[768,6,64]{0,2,1:T(8,128)} fusion(bf16[768,6,64]{0,2,1:T(8,128)(2,1)} %bitcast.252, bf16[768,6,64]{0,2,1:T(8,128)(2,1)} %bitcast.247, bf16[768,6,64]{0,2,1:T(8,128)(2,1)} %bitcast.250, f32[6,768]{1,0:T(8,128)S(1)} %bitcast.244, pred[768,768]{1,0:T(8,128)(4,1)} %iota_compare_fusion), kind=kOutput, calls=%fused_computation.20 | convolution fusion | flops 923664384 | bytes 3557376 | tf_op jit(solution)/shard_map/hts,shd->thd/dot_general | solution.py:127
  88.5 2.2 %multiply_reduce_fusion = (f32[768,6]{0,1:T(8,128)S(1)}, f32[768,6,64]{0,2,1:T(8,128)S(1)}) fusion(f32[768,6,64]{0,2,1:T(8,128)} %fusion.8, f32[768,6]{0,1:T(8,128)S(1)} %get-tuple-element.6, bf16[768,6,64]{0,2,1:T(8,128)(2,1)} %bitcast.248, bf16[8,6,64,64]{3,2,1,0:T(8,128)(2,1)S(1)} %all_gather.32, f32[6]{0:T(128)S(1)} %get-tuple-element.15, ...), kind=kOutput, calls=%fused_computation.36 | convolution fusion | flops 40103424 | bytes 3576132 | tf_op jit(solution)/shard_map/thd,hde->the/dot_general | solution.py:147
  90.8 1.6 %reshape.323 = f32[2,384,384]{1,0,2:T(2,128)} reshape(f32[768,6,64]{0,2,1:T(8,128)S(1)} %broadcast_multiply_fusion) | data formatting | bytes 2359296 | tf_op jit(solution)/shard_map/reshape | solution.py:150
  92.5 1.4 fusion.35
  93.9 20.2 %all_to_all.32 = bf16[2,384,384]{1,2,0:T(8,128)(2,1)S(1)} all-to-all(bf16[2,384,384]{1,2,0:T(8,128)(2,1)S(1)} %fusion.35), channel_id=1, replica_groups=mesh['sp_0'=8,'sp_1'=4,'fs'=4,'tp'=2] {'tp'}, dimensions={0} | all-to-all | bytes 1179648 | tf_op jit(solution)/shard_map/all_to_all | solution.py:156
  114.0 5.1 %fusion.140 = f32[384,2048]{1,0:T(8,128)} fusion(bf16[384,768]{0,1:T(8,128)(2,1)S(1)} %bitcast.241, bf16[768,2048]{1,0:T(8,128)(2,1)} %all-gather.9.cloned.1.call-done), kind=kOutput, calls=%fused_computation.194 | convolution fusion | flops 1207959552 | bytes 6881280 | tf_op jit(solution)/shard_map/dot_general | solution.py:159
  119.2 2.3 %fusion.14 = bf16[768,384]{0,1:T(8,128)(2,1)} fusion(bf16[2048,384]{1,0:T(8,128)(2,1)S(1)} %copy-done.7, bf16[1,768,2048]{2,1,0:T(8,128)(2,1)S(1)} %copy-done.2, f32[2048]{0:T(1024)S(1)} %copy-done.10, f32[768]{0:T(1024)S(1)} %add_rsqrt_fusion.1), kind=kOutput, calls=%fused_computation.27 | convolution fusion | flops 1213267968 | bytes 5319680 | tf_op jit(solution)/shard_map/dot_general | solution.py:104
  123.2 2.4 %reshape.324 = bf16[6,128,2,3,64]{1,0,4,3,2:T(8,128)(2,1)} reshape(bf16[768,384]{0,1:T(8,128)(2,1)} %fusion.14) | data formatting | bytes 1179648 | tf_op jit(solution)/shard_map/reshape | solution.py:55
  125.6 3.3 %collective-permute-start = (bf16[128,128]{1,0:T(8,128)(2,1)S(1)}, bf16[128,128]{1,0:T(8,128)(2,1)S(1)}, u32[]{:S(2)}, u32[]{:S(2)}) collective-permute-start(bf16[128,128]{1,0:T(8,128)(2,1)S(1)} %slice.185), channel_id=1, source_target_pairs={{0,8},{8,16},{16,24},{24,32},{32,40},{40,48},{48,56},{56,64},{64,7... | collective-permute-start | bytes 98312 | tf_op jit(solution)/shard_map/ppermute | solution.py:46
  130.5 2.0 %fusion.3 = (f32[2,3,6,128]{3,1,2,0:T(4,128)S(1)}, f32[2,6,256,128,3]{3,2,4,1,0:T(8,128)S(1)}) fusion(pred[6,128,256]{1,2,0:T(8,128)(4,1)S(1)} %broadcast_and_fusion, bf16[6,128,2,3,64]{1,0,4,3,2:T(8,128)(2,1)} %reshape.324, bf16[6,128,2,64]{1,3,0,2:T(8,128)(2,1)S(1)} %copy.49, bf16[6,128,2,64]{1,3,0,2:T(8,128)(2,1)S(1)} %copy.48), kind=kOutput, calls=%fused_computation.9 | convolution fusion | flops 155315712 | bytes 5916672 | tf_op jit(solution)/shard_map/nqhgd,nkhd->hgnqk/dot_general | solution.py:60
  133.8 1.4 fusion.26
  136.9 4.6 %all-to-all-start.1 = ((bf16[2,384,384]{1,2,0:T(8,128)(2,1)}), bf16[2,384,384]{1,2,0:T(8,128)(2,1)S(1)}, u32[]{:S(2)}, u32[]{:S(2)}) async-start(bf16[2,384,384]{1,2,0:T(8,128)(2,1)} %copy.54), calls=%async_computation.1 | async-start | bytes 1179648 | tf_op jit(solution)/shard_map/all_to_all | solution.py:157
  141.6 1.4 all-to-all-done.1
  143.0 5.4 %fusion.4 = bf16[1,384,2048]{2,1,0:T(8,128)(2,1)} fusion(f32[384,2048]{1,0:T(8,128)} %fusion.140, bf16[384,768]{0,1:T(8,128)(2,1)S(1)} %bitcast.242, bf16[768,2048]{1,0:T(8,128)(2,1)} %all-gather.11.cloned.1.call-done), kind=kOutput, calls=%fused_computation.11 | convolution fusion | flops 1209532416 | bytes 8454144 | tf_op jit(solution)/shard_map/dot_general | solution.py:163
  (91 shorter events, 13.4 us)
Async XLA Ops:
  6.5 38.2 %copy-start = (bf16[2048,384]{1,0:T(8,128)(2,1)S(1)}, bf16[2048,384]{1,0:T(8,128)(2,1)}, u32[]{:S(2)}) copy-start(bf16[2048,384]{1,0:T(8,128)(2,1)} %param.16) | copy-start | bytes 4718596
  6.5 4.6 %copy-start.14 = (u32[256]{0:T(256)S(1)}, u32[256]{0:T(256)}, u32[]{:S(2)}) copy-start(u32[256]{0:T(256)} %constant.64) | copy-start | bytes 3076
  6.5 2.2 %copy-start.3 = (f32[1,6,768]{2,0,1:T(1,128)S(1)}, f32[1,6,768]{2,0,1:T(1,128)}, u32[]{:S(2)}) copy-start(f32[1,6,768]{2,0,1:T(1,128)} %param.21) | copy-start | bytes 55300
  6.5 32.3 %copy-start.11 = (f32[6]{0:T(128)S(1)}, f32[6]{0:T(128)}, u32[]{:S(2)}) copy-start(f32[6]{0:T(128)} %param.23) | copy-start | bytes 76
  6.5 32.9 %all-gather.7.cloned.1.call-start = ((), (), s32[]{:S(2)}) async-start(), calls=%async_computation.2 | async-start | bytes 4718592 | tf_op jit(solution)/shard_map/all_gather | solution.py:101
  7.3 106.8 %all-gather.9.cloned.1.call-start = ((), (), s32[]{:S(2)}) async-start(), calls=%async_computation.3 | async-start | bytes 4718592 | tf_op jit(solution)/shard_map/all_gather | solution.py:161
  8.0 34.1 %copy-start.8 = (bf16[2048,128]{1,0:T(8,128)(2,1)S(1)}, bf16[2048,128]{1,0:T(8,128)(2,1)}, u32[]{:S(2)}) copy-start(bf16[2048,128]{1,0:T(8,128)(2,1)} %param.19) | copy-start | bytes 1572868
  8.0 34.1 %copy-start.10 = (f32[2048]{0:T(1024)S(1)}, f32[2048]{0:T(1024)}, u32[]{:S(2)}) copy-start(f32[2048]{0:T(1024)} %param.14) | copy-start | bytes 24580
  8.0 133.5 %all-gather.11.cloned.1.call-start = ((), (), s32[]{:S(2)}) async-start(), calls=%async_computation.4 | async-start | bytes 4718592 | tf_op jit(solution)/shard_map/all_gather | solution.py:165
  39.4 2.8 %copy-start.1 = (bf16[1,768,2048]{2,1,0:T(8,128)(2,1)S(1)}, bf16[1,768,2048]{2,1,0:T(8,128)(2,1)}, u32[]{:S(2)}) copy-start(bf16[1,768,2048]{2,1,0:T(8,128)(2,1)} %all-gather.7.cloned.1.call-done) | copy-start | bytes 9437188
  43.3 2.9 %copy-start.5 = (bf16[2048,384]{1,0:T(8,128)(2,1)S(1)}, bf16[2048,384]{1,0:T(8,128)(2,1)}, u32[]{:S(2)}) copy-start(bf16[2048,384]{1,0:T(8,128)(2,1)} %param.17) | copy-start | bytes 4718596
  43.3 86.0 %collective-permute-start.1 = (bf16[128,128]{1,0:T(8,128)(2,1)S(1)}, bf16[128,128]{1,0:T(8,128)(2,1)S(1)}, u32[]{:S(2)}, u32[]{:S(2)}) collective-permute-start(bf16[128,128]{1,0:T(8,128)(2,1)S(1)} %slice.186), channel_id=1, source_target_pairs={{0,8},{8,16},{16,24},{24,32},{32,40},{40,48},{48,56},{56,64},{64,7... | collective-permute-start | bytes 98312 | tf_op jit(solution)/shard_map/ppermute | solution.py:46
  46.2 1.5 copy-start.12
  47.6 32.3 %copy-start.13 = (bf16[768,384]{0,1:T(8,128)(2,1)}, bf16[768,384]{0,1:T(8,128)(2,1)S(1)}, u32[]{:S(2)}) copy-start(bf16[768,384]{0,1:T(8,128)(2,1)S(1)} %fusion.11) | copy-start | bytes 1769476
  47.6 30.0 %copy-start.6 = (bf16[2048,384]{1,0:T(8,128)(2,1)S(1)}, bf16[2048,384]{1,0:T(8,128)(2,1)}, u32[]{:S(2)}) copy-start(bf16[2048,384]{1,0:T(8,128)(2,1)} %param.15) | copy-start | bytes 4718596
  90.7 1.8 %copy-start.4 = (f32[384]{0:T(512)S(1)}, f32[384]{0:T(512)}, u32[]{:S(2)}) copy-start(f32[384]{0:T(512)} %param.22) | copy-start | bytes 4612
  114.0 5.1 %copy-start.2 = (bf16[1,768,2048]{2,1,0:T(8,128)(2,1)S(1)}, bf16[1,768,2048]{2,1,0:T(8,128)(2,1)}, u32[]{:S(2)}) copy-start(bf16[1,768,2048]{2,1,0:T(8,128)(2,1)} %all-gather.7.cloned.1.call-done) | copy-start | bytes 9437188
  114.0 5.1 %copy-start.7 = (bf16[2048,384]{1,0:T(8,128)(2,1)S(1)}, bf16[2048,384]{1,0:T(8,128)(2,1)}, u32[]{:S(2)}) copy-start(bf16[2048,384]{1,0:T(8,128)(2,1)} %param.18) | copy-start | bytes 4718596
  119.2 2.3 %copy-start.9 = (bf16[2048,128]{1,0:T(8,128)(2,1)S(1)}, bf16[2048,128]{1,0:T(8,128)(2,1)}, u32[]{:S(2)}) copy-start(bf16[2048,128]{1,0:T(8,128)(2,1)} %param.20) | copy-start | bytes 1572868
  125.6 4.3 %collective-permute-start = (bf16[128,128]{1,0:T(8,128)(2,1)S(1)}, bf16[128,128]{1,0:T(8,128)(2,1)S(1)}, u32[]{:S(2)}, u32[]{:S(2)}) collective-permute-start(bf16[128,128]{1,0:T(8,128)(2,1)S(1)} %slice.185), channel_id=1, source_target_pairs={{0,8},{8,16},{16,24},{24,32},{32,40},{40,48},{48,56},{56,64},{64,7... | collective-permute-start | bytes 98312 | tf_op jit(solution)/shard_map/ppermute | solution.py:46
  136.9 6.0 %all-to-all-start.1 = ((bf16[2,384,384]{1,2,0:T(8,128)(2,1)}), bf16[2,384,384]{1,2,0:T(8,128)(2,1)S(1)}, u32[]{:S(2)}, u32[]{:S(2)}) async-start(bf16[2,384,384]{1,2,0:T(8,128)(2,1)} %copy.54), calls=%async_computation.1 | async-start | bytes 1179648 | tf_op jit(solution)/shard_map/all_to_all | solution.py:157
Sparse Core Ops, SparseCore 0:
  9.1 21.9 all-gather.6
  32.9 18.7 all-gather.8
  53.5 18.7 all-gather.10
where the time goes:
time: 156 us; the launch traced here: 155 us
  blocking collectives  74.6 us (48%)
  matrix products  34.4 us (22%)
  between operations  14.2 us (9%)
  starting transfers between devices  9.45 us (6%)
  other arithmetic  9.42 us (6%)
  local copies, waits for them, and re-layouts  9.37 us (6%)
  waiting for transfers between devices  3.52 us (2%)
    all_gather x3, blocking collectives, entering(): lax.all_gather(part.astype(kind), axis)  44.9 us
    all_to_all x1, blocking collectives, shards(): lax.all_to_all(ret_out, 'tp', split_axis=0, concat_axis=1, tiled=True)  20.2 us
    unnamed x1, blocking collectives  9.52 us
    dot_general x6, matrix products, shards(): jnp.dot(scaled, weight, preferred_element_type=jnp.float32)  9.35 us
    dot_general x1, matrix products, shards(): jnp.einsum('hts,shd->thd', weights, shaped_v, preferred_element_type=jnp....  8.58 us
    dot_general x1, matrix products, shards(): jnp.dot(att_rows, lax.all_gather(out_att, 'tp', axis=0, tiled=True), pref...  5.42 us
    dot_general x1, matrix products, shards(): jnp.dot(ret_rows, lax.all_gather(retentive_exit_matrix, 'tp', axis=0, til...  5.11 us
    ppermute x2, starting transfers between devices, passed_along(): return lax.ppermute(value, axis, pairs)  4.72 us
  transfers between devices with their start and end apart: 6, of which 1 were waited for; matrix products, arithmetic and copies ran while one was open for 31% of the time, Pallas kernels for 0%

commit v1 on v0

v1 whole, which is shorter than its diff:
```python
import functools

import jax
import jax.numpy as jnp
from jax import lax
from jax.experimental import pallas as pl
from jax.experimental.pallas import tpu as pltpu
from jax.sharding import PartitionSpec as P

EPS = 1e-06
D = 2048
T = 768
HALF = 384
C = 128
NC = 6
NEG = float("-inf")
f32 = jnp.float32
bf16 = jnp.bfloat16


def dot(a, b):
    return jnp.dot(a, b, preferred_element_type=f32)


def dot_t(a, b):
    return lax.dot_general(a, b, (((1,), (1,)), ((), ())), preferred_element_type=f32)


def t_dot(a, b):
    return lax.dot_general(a, b, (((0,), (0,)), ((), ())), preferred_element_type=f32)


def split3(x):
    a = x.astype(bf16).astype(f32)
    r = x - a
    b = r.astype(bf16).astype(f32)
    return a, b, (r - b).astype(bf16).astype(f32)


def iota(shape, dim):
    return lax.broadcasted_iota(jnp.int32, shape, dim)


def kernel(
    tok, gain, wrq, wrk, wrv, waq, wak, wav, ld, rgain, sink, wre, wao,
    out,
    gain_v, rgain_v, sink_v, ld_v,
    tok_o, tok_p, sc_o, ssq,
    wkv, wq, wa, acc_kv, acc_q, acc_a,
    kv, qb, akv, qs,
    lcrow, lch, el, tots, et, st, inner,
    wmask, biasc,
    st_a, buf_a, l_a, buf_al, g_b, buf_b, l_b, buf_bl, s_c, buf_c,
    wo, att, att_p, ret, ret_p, oacc,
    lsem, tsem, trec, wsem, wrec, hsem, hrec,
    asem, arec, alsem, alrec, bsem, brec, blsem, blrec, csem, crec, osem, orec,
):
    sp = lax.axis_index("sp")
    tp = lax.axis_index("tp")
    y = lax.rem(sp, 4)
    z = lax.div(sp, 4)
    other = 1 - tp
    peer = {"tp": other}
    y_at = [lax.rem(y + d, 4) for d in range(4)]
    z_at = [lax.rem(z + d, 8) for d in range(8)]

    def at_y(d):
        return {"sp": z * 4 + y_at[d]}

    def at_z(d):
        return {"sp": z_at[d] * 4 + y}

    nxt = {"sp": lax.rem(sp + 1, 32)}
    prv = {"sp": lax.rem(sp + 31, 32)}

    barrier = pltpu.get_barrier_semaphore()
    greet = [peer] + [at_y(d) for d in range(1, 4)] + [at_z(d) for d in range(1, 8)] + [prv]
    for who in greet:
        pl.semaphore_signal(barrier, inc=1, device_id=who, device_id_type=pl.DeviceIdType.MESH)

    local = []

    def load(src, dst):
        cp = pltpu.make_async_copy(src, dst, lsem.at[len(local)])
        cp.start()
        local.append(cp)
        return cp

    own = pl.ds(pl.multiple_of(tp * 1024, 1024), 1024)
    oth = pl.ds(pl.multiple_of(other * 1024, 1024), 1024)
    here, there = pl.ds(0, 1024), pl.ds(1024, 1024)

    def load2(a, b, rows, dst, to, w):
        return [load(a.at[rows], dst.at[to, pl.ds(0, w)]), load(b.at[rows], dst.at[to, pl.ds(w, w)])]

    c_tok = load(tok.at[0], tok_o)
    c_ld = [load(ld.at[h], ld_v.at[pl.ds(h, 1)]) for h in range(6)]
    c_gain = load(gain, gain_v)
    c_kv = load2(wrk, wrv, own, wkv, here, 384)

    lane1 = iota((1, 128), 1)
    m0 = jnp.where(lane1 < 64, 1.0, 0.0).astype(bf16)
    m1 = jnp.where(lane1 < 64, 0.0, 1.0).astype(bf16)
    wmask[0:C] = jnp.where(iota((C, C), 0) > iota((C, C), 1), 1.0, 0.0).astype(bf16)
    wmask[C:] = jnp.where(iota((C, C), 0) > iota((C, C), 1), 0.0, 1.0).astype(bf16)
    biasc[...] = jnp.where(iota((C, C), 0) >= iota((C, C), 1), 0.0, NEG)

    for cp in c_ld:
        cp.wait()
    raw = ld_v[...]
    rows48 = jnp.concatenate([raw[:, c * C:(c + 1) * C] for c in range(NC)], axis=0)
    rows48 = jnp.where(lax.rem(iota((48, C), 0), 8) < 6, rows48, 0.0)
    upper = jnp.where(iota((C, C), 0) <= iota((C, C), 1), 1.0, 0.0).astype(bf16)
    parts = jnp.concatenate(split3(rows48), axis=0).astype(bf16)
    summed = dot(parts, upper)
    lc = summed[0:48] + summed[48:96] + summed[96:144]
    lcrow[...] = lc
    sr, sl = lax.rem(iota((24, 1152), 0), 8), iota((24, 1152), 1)
    head_of = jnp.where(sl < 384, lax.div(sl, 64), lax.div(sl - 384, 128))
    sel = jnp.where(sr == head_of, 1.0, 0.0).astype(bf16)
    before = jnp.zeros((1, 384), f32)
    for c in range(NC):
        p3 = jnp.concatenate(split3(lc[c * 8:(c + 1) * 8]), axis=0).astype(bf16)
        cols = t_dot(p3, sel)
        lch[pl.ds(c * C, C)] = cols[:, 384:]
        el[pl.ds(c * C, C)] = cols[:, :384]
        last = cols[C - 1:C, :384]
        tots[c:c + 1] = last
        et[c:c + 1] = jnp.exp(before)
        before = before + last
    for p in range(3):
        l_a[p:p + 1] = before[:, p * 128:(p + 1) * 128]

    c_gain.wait()
    c_tok.wait()
    c_a = load2(wak, wav, own, wa, here, 128)
    c_q = load2(wrq, waq, own, wq, here, 384)
    g_o = gain_v[:, own]
    g_p = gain_v[:, oth]

    def scale_rows(src, r0, g):
        x = src[pl.ds(r0, 64)].astype(f32)
        sq = x * x
        part = sq[:, 0:128]
        for j in range(1, 8):
            part = part + sq[:, j * 128:(j + 1) * 128]
        return (x * g).astype(bf16), part

    def own_rows(i, carry):
        r0 = pl.multiple_of(i * 64, 64)
        s, part = scale_rows(tok_o, r0, g_o)
        sc_o[pl.ds(r0, 64)] = s
        ssq[pl.ds(r0, 64)] = part
        return carry

    lax.fori_loop(0, T // 64, own_rows, 0)

    pl.semaphore_wait(barrier, len(greet))

    t_cp = []
    for r in range(2):
        rows = pl.ds(r * HALF, HALF)
        cp = pltpu.make_async_remote_copy(
            src_ref=tok.at[0, rows], dst_ref=tok_p.at[rows], send_sem=tsem.at[r], recv_sem=trec.at[r],
            device_id=peer, device_id_type=pl.DeviceIdType.MESH)
        cp.start()
        t_cp.append(cp)
    w_cp = []
    for i, w in enumerate((wre, wao)):
        cp = pltpu.make_async_remote_copy(
            src_ref=w, dst_ref=wo.at[i, pl.ds(384, 384)], send_sem=wsem.at[i], recv_sem=wrec.at[i],
            device_id=peer, device_id_type=pl.DeviceIdType.MESH)
        cp.start()
        w_cp.append(cp)

    c_kv2 = load2(wrk, wrv, oth, wkv, there, 384)
    c_a2 = load2(wak, wav, oth, wa, there, 128)
    c_q2 = load2(wrq, waq, oth, wq, there, 384)
    c_small = [load(rgain, rgain_v), load(sink, sink_v)]
    c_wo = [load(wre, wo.at[0, pl.ds(0, 384)]), load(wao, wo.at[1, pl.ds(0, 384)])]

    def first_half(acc, w):
        for r in range(2):
            rows = pl.ds(r * HALF, HALF)
            acc[rows] = dot(sc_o[rows], w[here])

    def wait_all(cps):
        for cp in cps:
            cp.wait()

    wait_all(c_kv)
    first_half(acc_kv, wkv)
    wait_all(c_a)
    first_half(acc_a, wa)
    wait_all(c_q)
    first_half(acc_q, wq)

    inv = [None, None]
    wait_all(c_kv2)
    for r in range(2):
        t_cp[r].wait_recv()

        def peer_rows(i, carry):
            r0 = pl.multiple_of(r * HALF + i * 64, 64)
            s, part = scale_rows(tok_p, r0, g_p)
            tok_p[pl.ds(r0, 64)] = s
            total = jnp.sum(ssq[pl.ds(r0, 64)] + part, axis=1, keepdims=True)
            ssq[pl.ds(r0, 64)] = jnp.broadcast_to(lax.rsqrt(total / D + EPS), (64, 128))
            return carry

        lax.fori_loop(0, HALF // 64, peer_rows, 0)
        rows = pl.ds(r * HALF, HALF)
        res = acc_kv[rows] + dot(tok_p[rows], wkv[there])
        kv[rows] = (res * ssq[rows, 0:1]).astype(bf16)

    lo = iota((64, 128), 1) < 64
    s_p = [jnp.zeros((64, 128), f32) for _ in range(3)]
    for c in range(NC):
        rows = pl.ds(c * C, C)
        tot = tots[c:c + 1]
        for p in range(3):
            cols = pl.ds(p * 128, 128)
            tp_ = tot[:, p * 128:(p + 1) * 128]
            lcp = el[rows, cols]
            kd = (kv[rows, cols].astype(f32) * jnp.exp(tp_ - lcp)).astype(bf16)
            m = t_dot(kd, kv[rows, pl.ds(384 + p * 128, 128)])
            comp = jnp.where(lo, m[0:64], m[64:128])
            st[c, p] = s_p[p].astype(bf16)
            s_p[p] = jnp.exp(tp_) * s_p[p] + comp
    for p in range(3):
        for q in range(4):
            st_a[q, p] = s_p[p][q * 16:(q + 1) * 16].astype(bf16)

    a_cp, al_cp = [], []

    def send(src, dst, ss, rs, who, group):
        cp = pltpu.make_async_remote_copy(
            src_ref=src, dst_ref=dst, send_sem=ss, recv_sem=rs, device_id=who,
            device_id_type=pl.DeviceIdType.MESH)
        cp.start()
        group.append(cp)

    def arrived(src, dst, ss, rs, who):
        pltpu.make_async_remote_copy(
            src_ref=src, dst_ref=dst, send_sem=ss, recv_sem=rs, device_id=who,
            device_id_type=pl.DeviceIdType.MESH).wait_recv()

    for d in range(1, 4):
        send(st_a.at[y_at[d]], buf_a.at[y], asem.at[d - 1], arec.at[y], at_y(d), a_cp)
        send(l_a, buf_al.at[y], alsem.at[d - 1], alrec.at[y], at_y(d), al_cp)
    buf_a[y] = st_a[y]
    buf_al[y] = l_a[...]

    wait_all(c_a2)
    for r in range(2):
        rows = pl.ds(r * HALF, HALF)
        res = acc_a[rows] + dot(tok_p[rows], wa[there])
        akv[pl.ds(C + r * HALF, HALF)] = (res * ssq[rows, 0:1]).astype(bf16)
    halo = pltpu.make_async_remote_copy(
        src_ref=akv.at[pl.ds(T, C)], dst_ref=akv.at[pl.ds(0, C)], send_sem=hsem, recv_sem=hrec,
        device_id=nxt, device_id_type=pl.DeviceIdType.MESH)
    halo.start()
    wait_all(c_q2)
    for r in range(2):
        rows = pl.ds(r * HALF, HALF)
        res = acc_q[rows] + dot(tok_p[rows], wq[there])
        res = res * (ssq[rows, 0:1] * 0.125)
        qb[rows] = res[:, :384].astype(bf16)
        for p in range(3):
            two = res[:, 384 + p * 128:384 + (p + 1) * 128]
            swapped = pltpu.roll(two, 64, 1) if p != 1 else two
            for j in range(2):
                h = 2 * p + j
                val = ((swapped if h in (1, 4) else two).astype(bf16)) * (m0 if h < 3 else m1)
                for b in range(3):
                    qs[r * 3 + b, pl.ds(h * C, C)] = val[b * C:(b + 1) * C]

    def spread(s):
        return jnp.concatenate([s * m0, s * m1], axis=0)

    def ret_chunk(c, carry):
        rows = pl.ds(pl.multiple_of(c * C, C), C)
        past = et[pl.ds(c, 1)]
        lrows = lcrow[pl.ds(pl.multiple_of(c * 8, 8), 8)]
        for p in range(3):
            cols = pl.ds(p * 128, 128)
            q2, k2, v2 = qb[rows, cols], kv[rows, cols], kv[rows, pl.ds(384 + p * 128, 128)]
            ws = []
            for j, mj in enumerate((m0, m1)):
                h = 2 * p + j
                gap = lch[rows, pl.ds(h * 128, 128)] - lrows[h:h + 1] + biasc[...]
                ws.append((dot_t(q2 * mj, k2) * jnp.exp(gap)).astype(bf16))
            ex = jnp.exp(el[rows, cols])
            el[rows, cols] = ex * past[:, p * 128:(p + 1) * 128]
            ws.append((q2.astype(f32) * ex).astype(bf16))
            rhs = jnp.concatenate([v2 * m0, v2 * m1, spread(st[c, p])], axis=0)
            inner[rows, cols] = dot(jnp.concatenate(ws, axis=1), rhs)
        return carry

    lax.fori_loop(0, NC, ret_chunk, 0)

    for d in range(1, 4):
        arrived(st_a.at[0], buf_a.at[y_at[d]], asem.at[d - 1], arec.at[y_at[d]], at_y(d))
        arrived(l_a, buf_al.at[y_at[d]], alsem.at[d - 1], alrec.at[y_at[d]], at_y(d))
    b_cp, bl_cp = [], []
    for p in range(3):
        e = jnp.zeros((16, 128), f32)
        ltot = jnp.zeros((1, 128), f32)
        for yy in range(4):
            lyy = buf_al[yy][p:p + 1]
            e = jnp.exp(lyy) * e + buf_a[yy, p].astype(f32)
            ltot = ltot + lyy
        g_b[p] = e.astype(bf16)
        l_b[p:p + 1] = ltot
    for d in range(1, 8):
        send(g_b, buf_b.at[z], bsem.at[d - 1], brec.at[z], at_z(d), b_cp)
        send(l_b, buf_bl.at[z], blsem.at[d - 1], blrec.at[z], at_z(d), bl_cp)
    buf_b[z] = g_b[...]
    buf_bl[z] = l_b[...]

    wait_all(c_small)
    halo.wait_recv()
    sink_row = jnp.concatenate(
        [jnp.broadcast_to(sink_v[0:1, h:h + 1], (1, C)) for h in range(6)], axis=1)

    def att_block(i, half):
        n = half * 3 + i
        bandr = pl.ds(pl.multiple_of(n * C, C), 2 * C)
        edge = (n == 0) & (sp == 0)
        s = dot_t(akv[bandr, pl.ds(0, 128)], qs[n])
        is_own = iota((C, C), 0) <= iota((C, C), 1)
        ws, scale = [], []
        for h in range(6):
            hc = slice(h * C, (h + 1) * C)
            past = jnp.where(edge, NEG, s[:C, hc])
            v = jnp.where(is_own, s[C:, hc], past)
            sk = sink_row[:, hc]
            top = jnp.maximum(jnp.max(v, axis=0, keepdims=True), sk)
            e = jnp.exp(v - top)
            scale.append(1.0 / (jnp.sum(e, axis=0, keepdims=True) + jnp.exp(sk - top)))
            eb = e.astype(bf16)
            ws.append(jnp.concatenate([eb * wmask[0:C], eb * wmask[C:]], axis=0))
        o = t_dot(akv[bandr, pl.ds(128, 128)], jnp.concatenate(ws, axis=1))
        cols = pl.ds(pl.multiple_of(i * C, C), C)
        for h in range(6):
            r0 = 64 if h >= 3 else 0
            att[half, pl.ds(h * 64, 64), cols] = (
                o[r0:r0 + 64, h * C:(h + 1) * C] * scale[h]).astype(bf16)
        return half

    mine = pl.ds(pl.multiple_of(tp * HALF, HALF), HALF)
    theirs = pl.ds(pl.multiple_of(other * HALF, HALF), HALF)
    o_cp = []
    lax.fori_loop(0, 3, att_block, other)
    send(att.at[other], att_p, osem.at[0], orec.at[0], peer, o_cp)
    lax.fori_loop(0, 3, att_block, tp)

    for d in range(1, 8):
        arrived(g_b, buf_b.at[z_at[d]], bsem.at[d - 1], brec.at[z_at[d]], at_z(d))
        arrived(l_b, buf_bl.at[z_at[d]], blsem.at[d - 1], blrec.at[z_at[d]], at_z(d))
    for p in range(3):
        e = jnp.zeros((16, 128), f32)
        for zz in range(7):
            step = jnp.exp(buf_bl[zz][p:p + 1]) * e + buf_b[zz, p].astype(f32)
            e = jnp.where(zz < z, step, e)
        for yy in range(4):
            s_c[yy, p] = e.astype(bf16)
            e = jnp.exp(buf_al[yy][p:p + 1]) * e + buf_a[yy, p].astype(f32)
    c_cp = []
    for d in range(1, 4):
        send(s_c.at[y_at[d]], buf_c.at[y], csem.at[d - 1], crec.at[y], at_y(d), c_cp)
    buf_c[y] = s_c[y]

    wait_all(c_wo)
    w_cp[0].wait_recv()
    w_cp[1].wait_recv()
    o_cp[0].wait_recv()
    lhs = jnp.concatenate([att[tp], att_p[...]], axis=0)
    for j in range(4):
        cols = pl.ds(j * 512, 512)
        oacc[:, cols] = t_dot(lhs, wo[1, :, cols])

    for d in range(1, 4):
        arrived(s_c.at[0], buf_c.at[y_at[d]], csem.at[d - 1], crec.at[y_at[d]], at_y(d))
    big = [spread(jnp.concatenate([buf_c[q, p] for q in range(4)], axis=0)) for p in range(3)]
    ones_bd = jnp.where(
        lax.div(iota((128, 128), 0), 64) == lax.div(iota((128, 128), 1), 64), 1.0, 0.0).astype(bf16)

    def finish(rows):
        for p in range(3):
            cols = pl.ds(p * 128, 128)
            full = inner[rows, cols] + dot(qb[rows, cols], big[p]) * el[rows, cols]
            ms = dot((full * full).astype(bf16), ones_bd) * (1.0 / 64)
            ret[rows, cols] = (full * lax.rsqrt(ms + EPS) * rgain_v[cols].reshape(1, 128)).astype(bf16)

    finish(theirs)
    send(ret.at[theirs], ret_p, osem.at[1], orec.at[1], peer, o_cp)
    finish(mine)
    o_cp[1].wait_recv()
    lhs = jnp.concatenate([ret[mine], ret_p[...]], axis=1)
    for j in range(4):
        cols = pl.ds(j * 512, 512)
        out[0, :, cols] = (oacc[:, cols] + dot(lhs, wo[0, :, cols])).astype(bf16)

    for cp in t_cp + w_cp + a_cp + al_cp + b_cp + bl_cp + c_cp + o_cp + [halo]:
        cp.wait_send()


def shards(tokens, in_gain, ret_query, ret_key, ret_value, att_query, att_key, att_value,
           log_decay, ret_gain, sink_logit, retentive_exit_matrix, out_att):
    hbm = pl.BlockSpec(memory_space=pltpu.HBM)
    V = pltpu.VMEM
    DMA = pltpu.SemaphoreType.DMA
    scratch = [
        V((1, D), f32), V((384,), f32), V((1, 6), f32), V((8, T), f32),
        V((T, 1024), bf16), V((T, 1024), bf16), V((T, 1024), bf16), V((T, 128), f32),
        V((D, 768), bf16), V((D, 768), bf16), V((D, 256), bf16),
        V((T, 768), f32), V((T, 768), f32), V((T, 256), f32),
        V((T, 768), bf16), V((T, 384), bf16), V((T + C, 256), bf16), V((NC, 768, 128), bf16),
        V((48, 128), f32), V((T, 768), f32), V((T, 384), f32), V((8, 384), f32), V((8, 384), f32),
        V((NC, 3, 64, 128), bf16), V((T, 384), f32),
        V((2 * C, C), bf16), V((C, C), f32),
        V((4, 3, 16, 128), bf16), V((4, 3, 16, 128), bf16), V((8, 128), f32), V((4, 8, 128), f32),
        V((3, 16, 128), bf16), V((8, 3, 16, 128), bf16), V((8, 128), f32), V((8, 8, 128), f32),
        V((4, 3, 16, 128), bf16), V((4, 3, 16, 128), bf16),
        V((2, 768, D), bf16), V((2, 384, HALF), bf16), V((384, HALF), bf16), V((T, 384), bf16),
        V((HALF, 384), bf16), V((HALF, D), f32),
        DMA((24,)), DMA((2,)), DMA((2,)), DMA((2,)), DMA((2,)), DMA(()), DMA(()),
        DMA((3,)), DMA((4,)), DMA((3,)), DMA((4,)), DMA((7,)), DMA((8,)), DMA((7,)), DMA((8,)),
        DMA((3,)), DMA((4,)), DMA((2,)), DMA((2,)),
    ]
    return pl.pallas_call(
        kernel,
        out_shape=jax.ShapeDtypeStruct((1, HALF, D), bf16),
        in_specs=[hbm] * 13,
        out_specs=pl.BlockSpec(memory_space=pltpu.VMEM),
        scratch_shapes=scratch,
        compiler_params=pltpu.CompilerParams(
            collective_id=0, has_side_effects=True, vmem_limit_bytes=48 * 1024 * 1024),
    )(*(pltpu.with_memory_space_constraint(arg, pltpu.HBM) for arg in (
        tokens, in_gain.reshape(1, D), ret_query, ret_key, ret_value, att_query, att_key, att_value,
        jnp.transpose(log_decay, (1, 0, 2)), ret_gain, sink_logit.reshape(1, 6), retentive_exit_matrix, out_att,
    )))


def solution(mesh):
    placed = (
        P("fs", "sp", "tp"), P(), P(None, "tp"), P(None, "tp"), P(None, "tp"), P(None, "tp"),
        P(None, "tp"), P(None, "tp"), P("fs", "tp", "sp"), P("tp"), P("tp"), P("tp", None), P("tp", None),
    )
    return jax.shard_map(
        shards, mesh=mesh, in_specs=placed, out_specs=P("fs", ("sp", "tp"), None), check_vma=False)
```

time: 156 us -> 37.1 us (0.24)
  blocking collectives: 74.6 us -> 0 us
  Pallas kernels: 0 us -> 35.9 us
  matrix products: 34.4 us -> 0 us
  between operations: 14.2 us -> 0.01 us
  starting transfers between devices: 9.45 us -> 0 us
  other arithmetic: 9.42 us -> 0 us
  local copies, waits for them, and re-layouts: 9.37 us -> 1.15 us
  waiting for transfers between devices: 3.52 us -> 0 us
    all_gather x3 -> x0, blocking collectives: 44.9 us -> none  [entering(): lax.all_gather(part.astype(kind), axis)]
    pallas_call x0 -> x1, Pallas kernels: none -> 35.9 us  [shards(): pl.pallas_call(kernel, out_shape=jax.ShapeDtypeStruct((1, HALF, D), bf16)...]
    dot_general x13 -> x0, matrix products: 34.4 us -> none  [the longest x6 9.35 us: shards(): jnp.dot(scaled, weight, preferred_element_type=jnp.float32)]
    all_to_all x1 -> x0, blocking collectives: 20.2 us -> none  [shards(): lax.all_to_all(ret_out, 'tp', split_axis=0, concat_axis=1, tiled=True)]
    unnamed x1 -> x0, blocking collectives: 9.52 us -> none
    ppermute x2 -> x0, starting transfers between devices: 4.72 us -> none  [passed_along(): return lax.ppermute(value, axis, pairs)]
    all_to_all x1 -> x0, starting transfers between devices: 4.62 us -> none  [shards(): lax.all_to_all(att_out, 'tp', split_axis=0, concat_axis=1, tiled=True)]
    reshape x3 -> x0, local copies, waits for them, and re-layouts: 4.07 us -> none  [the longest x1 2.43 us: attend_window(): shaped_q = query_rows.reshape(blocks, WINDOW, heads_kv, group, HEAD_DIM)]
  transfers between devices with their start and end apart: 6 -> 0, of which waited for: 1 -> 0; matrix products, arithmetic and copies ran while one was open for 31% -> 0% of each run, Pallas kernels for 0% -> 0%
where the time goes in v1:
time: 37.1 us; the launch traced here: 37 us
  Pallas kernels  35.9 us (97%)
  local copies, waits for them, and re-layouts  1.15 us (3%)
    pallas_call x1, Pallas kernels, shards(): pl.pallas_call(kernel, out_shape=jax.ShapeDtypeStruct((1, HALF, D), bf16)...  35.9 us
    unnamed x1, local copies, waits for them, and re-layouts  1.15 us

profile of v1, /device:TPU:1, one launch (start us, length us, event | category | flops | bytes accessed | tf_op | source)
XLA Modules:
  0.0 37.0 jit_solution(17666822009813017248)
XLA Ops:
  0.0 35.9 %shard_map.127 = bf16[1,384,2048]{2,1,0:T(8,128)(2,1)S(1)} custom-call(bf16[1,768,1024]{2,1,0:T(8,128)(2,1)} %tok.1, f32[1,2048]{1,0:T(1,128)} %bitcast.4, bf16[2048,384]{1,0:T(8,128)(2,1)} %wrq.1, bf16[2048,384]{1,0:T(8,128)(2,1)} %wrk.1, bf16[2048,384]{1,0:T(8,128)(2,1)} %wrv.1, bf16[2048,384]{1,0:T(8,128)(2,1)} %waq.1, bf16[2048,128]{1,0:T(8,128)(2,1)} %wak.1, ...), custom_call_target="tpu_custom_call" | custom-call | tf_op jit(solution)/shard_map/pallas_call | solution.py:432
  35.9 1.1 %copy.15 = bf16[1,384,2048]{2,1,0:T(8,128)(2,1)} copy(bf16[1,384,2048]{2,1,0:T(8,128)(2,1)S(1)} %shard_map.127) | data formatting | bytes 3145728

commit v2 on v1

--- a/solution.py
+++ b/solution.py
@@ -46,7 +46,7 @@
     out,
     gain_v, rgain_v, sink_v, ld_v,
     tok_o, tok_p, sc_o, ssq,
-    wkv, wq, wa, acc_kv, acc_q, acc_a,
+    wkv, wq, wa, acc_kv, acc_a,
     kv, qb, akv, qs,
     lcrow, lch, el, tots, et, st, inner,
     wmask, biasc,
@@ -192,8 +192,6 @@
     first_half(acc_kv, wkv)
     wait_all(c_a)
     first_half(acc_a, wa)
-    wait_all(c_q)
-    first_half(acc_q, wq)
 
     inv = [None, None]
     wait_all(c_kv2)
@@ -260,10 +258,10 @@
         src_ref=akv.at[pl.ds(T, C)], dst_ref=akv.at[pl.ds(0, C)], send_sem=hsem, recv_sem=hrec,
         device_id=nxt, device_id_type=pl.DeviceIdType.MESH)
     halo.start()
-    wait_all(c_q2)
+    wait_all(c_q + c_q2)
     for r in range(2):
         rows = pl.ds(r * HALF, HALF)
-        res = acc_q[rows] + dot(tok_p[rows], wq[there])
+        res = dot(jnp.concatenate([sc_o[rows], tok_p[rows]], axis=1), wq[...])
         res = res * (ssq[rows, 0:1] * 0.125)
         qb[rows] = res[:, :384].astype(bf16)
         for p in range(3):
@@ -278,7 +276,8 @@
     def spread(s):
         return jnp.concatenate([s * m0, s * m1], axis=0)
 
-    def ret_chunk(c, carry):
+    def ret_chunk(i, carry):
+        c = lax.rem(other * 3 + i, NC)
         rows = pl.ds(pl.multiple_of(c * C, C), C)
         past = et[pl.ds(c, 1)]
         lrows = lcrow[pl.ds(pl.multiple_of(c * 8, 8), 8)]
@@ -297,7 +296,6 @@
             inner[rows, cols] = dot(jnp.concatenate(ws, axis=1), rhs)
         return carry
 
-    lax.fori_loop(0, NC, ret_chunk, 0)
 
     for d in range(1, 4):
         arrived(st_a.at[0], buf_a.at[y_at[d]], asem.at[d - 1], arec.at[y_at[d]], at_y(d))
@@ -354,6 +352,7 @@
     lax.fori_loop(0, 3, att_block, other)
     send(att.at[other], att_p, osem.at[0], orec.at[0], peer, o_cp)
     lax.fori_loop(0, 3, att_block, tp)
+    lax.fori_loop(0, 4, ret_chunk, 0)
 
     for d in range(1, 8):
         arrived(g_b, buf_b.at[z_at[d]], bsem.at[d - 1], brec.at[z_at[d]], at_z(d))
@@ -371,6 +370,8 @@
         send(s_c.at[y_at[d]], buf_c.at[y], csem.at[d - 1], crec.at[y], at_y(d), c_cp)
     buf_c[y] = s_c[y]
 
+    lax.fori_loop(4, NC, ret_chunk, 0)
+
     wait_all(c_wo)
     w_cp[0].wait_recv()
     w_cp[1].wait_recv()
@@ -396,11 +397,13 @@
     finish(theirs)
     send(ret.at[theirs], ret_p, osem.at[1], orec.at[1], peer, o_cp)
     finish(mine)
-    o_cp[1].wait_recv()
-    lhs = jnp.concatenate([ret[mine], ret_p[...]], axis=1)
     for j in range(4):
         cols = pl.ds(j * 512, 512)
-        out[0, :, cols] = (oacc[:, cols] + dot(lhs, wo[0, :, cols])).astype(bf16)
+        oacc[:, cols] += dot(ret[mine], wo[0, 0:384, cols])
+    o_cp[1].wait_recv()
+    for j in range(4):
+        cols = pl.ds(j * 512, 512)
+        out[0, :, cols] = (oacc[:, cols] + dot(ret_p[...], wo[0, 384:768, cols])).astype(bf16)
 
     for cp in t_cp + w_cp + a_cp + al_cp + b_cp + bl_cp + c_cp + o_cp + [halo]:
         cp.wait_send()
@@ -415,7 +418,7 @@
         V((1, D), f32), V((384,), f32), V((1, 6), f32), V((8, T), f32),
         V((T, 1024), bf16), V((T, 1024), bf16), V((T, 1024), bf16), V((T, 128), f32),
         V((D, 768), bf16), V((D, 768), bf16), V((D, 256), bf16),
-        V((T, 768), f32), V((T, 768), f32), V((T, 256), f32),
+        V((T, 768), f32), V((T, 256), f32),
         V((T, 768), bf16), V((T, 384), bf16), V((T + C, 256), bf16), V((NC, 768, 128), bf16),
         V((48, 128), f32), V((T, 768), f32), V((T, 384), f32), V((8, 384), f32), V((8, 384), f32),
         V((NC, 3, 64, 128), bf16), V((T, 384), f32),

time: 37.1 us -> 34.7 us (0.935)
  Pallas kernels: 35.9 us -> 33.4 us
    pallas_call x1, Pallas kernels: 35.9 us -> 33.4 us  [shards(): pl.pallas_call(kernel, out_shape=jax.ShapeDtypeStruct((1, HALF, D), bf16)...]
where the time goes in v2:
time: 34.7 us; the launch traced here: 34.6 us
  Pallas kernels  33.4 us (96%)
  local copies, waits for them, and re-layouts  1.15 us (3%)
    pallas_call x1, Pallas kernels, shards(): pl.pallas_call(kernel, out_shape=jax.ShapeDtypeStruct((1, HALF, D), bf16)...  33.4 us
    unnamed x1, local copies, waits for them, and re-layouts  1.15 us

profile of v2, /device:TPU:1, one launch (start us, length us, event | category | flops | bytes accessed | tf_op | source)
XLA Modules:
  0.0 34.6 jit_solution(17879582766703900557)
XLA Ops:
  0.0 33.4 %shard_map.127 = bf16[1,384,2048]{2,1,0:T(8,128)(2,1)S(1)} custom-call(bf16[1,768,1024]{2,1,0:T(8,128)(2,1)} %tok.1, f32[1,2048]{1,0:T(1,128)} %bitcast.4, bf16[2048,384]{1,0:T(8,128)(2,1)} %wrq.1, bf16[2048,384]{1,0:T(8,128)(2,1)} %wrk.1, bf16[2048,384]{1,0:T(8,128)(2,1)} %wrv.1, bf16[2048,384]{1,0:T(8,128)(2,1)} %waq.1, bf16[2048,128]{1,0:T(8,128)(2,1)} %wak.1, ...), custom_call_target="tpu_custom_call" | custom-call | tf_op jit(solution)/shard_map/pallas_call | solution.py:435
  33.4 1.1 %copy.15 = bf16[1,384,2048]{2,1,0:T(8,128)(2,1)} copy(bf16[1,384,2048]{2,1,0:T(8,128)(2,1)S(1)} %shard_map.127) | data formatting | bytes 3145728

commit v3 on v2

--- a/solution.py
+++ b/solution.py
@@ -48,7 +48,7 @@
     tok_o, tok_p, sc_o, ssq,
     wkv, wq, wa, acc_kv, acc_a,
     kv, qb, akv, qs,
-    lcrow, lch, el, tots, et, st, inner,
+    lcrow, exr, frow, lch, el, tots, st, inner, gcol,
     wmask, biasc,
     st_a, buf_a, l_a, buf_al, g_b, buf_b, l_b, buf_bl, s_c, buf_c,
     wo, att, att_p, ret, ret_p, oacc,
@@ -96,14 +96,13 @@
     c_tok = load(tok.at[0], tok_o)
     c_ld = [load(ld.at[h], ld_v.at[pl.ds(h, 1)]) for h in range(6)]
     c_gain = load(gain, gain_v)
-    c_kv = load2(wrk, wrv, own, wkv, here, 384)
 
     lane1 = iota((1, 128), 1)
     m0 = jnp.where(lane1 < 64, 1.0, 0.0).astype(bf16)
     m1 = jnp.where(lane1 < 64, 0.0, 1.0).astype(bf16)
     wmask[0:C] = jnp.where(iota((C, C), 0) > iota((C, C), 1), 1.0, 0.0).astype(bf16)
     wmask[C:] = jnp.where(iota((C, C), 0) > iota((C, C), 1), 0.0, 1.0).astype(bf16)
-    biasc[...] = jnp.where(iota((C, C), 0) >= iota((C, C), 1), 0.0, NEG)
+    biasc[...] = jnp.where(iota((C, C), 0) <= iota((C, C), 1), 0.0, NEG)
 
     for cp in c_ld:
         cp.wait()
@@ -118,7 +117,9 @@
     sr, sl = lax.rem(iota((24, 1152), 0), 8), iota((24, 1152), 1)
     head_of = jnp.where(sl < 384, lax.div(sl, 64), lax.div(sl - 384, 128))
     sel = jnp.where(sr == head_of, 1.0, 0.0).astype(bf16)
+    exr[...] = jnp.exp(lc)
     before = jnp.zeros((1, 384), f32)
+    before8 = jnp.zeros((8, 1), f32)
     for c in range(NC):
         p3 = jnp.concatenate(split3(lc[c * 8:(c + 1) * 8]), axis=0).astype(bf16)
         cols = t_dot(p3, sel)
@@ -126,13 +127,16 @@
         el[pl.ds(c * C, C)] = cols[:, :384]
         last = cols[C - 1:C, :384]
         tots[c:c + 1] = last
-        et[c:c + 1] = jnp.exp(before)
         before = before + last
+        lc8 = lc[c * 8:(c + 1) * 8]
+        frow[c * 8:(c + 1) * 8] = jnp.exp(lc8 + before8)
+        before8 = before8 + lc8[:, C - 1:C]
     for p in range(3):
         l_a[p:p + 1] = before[:, p * 128:(p + 1) * 128]
 
     c_gain.wait()
     c_tok.wait()
+    c_kv = load2(wrk, wrv, own, wkv, here, 384)
     c_a = load2(wak, wav, own, wa, here, 128)
     c_q = load2(wrq, waq, own, wq, here, 384)
     g_o = gain_v[:, own]
@@ -161,10 +165,48 @@
     for r in range(2):
         rows = pl.ds(r * HALF, HALF)
         cp = pltpu.make_async_remote_copy(
-            src_ref=tok.at[0, rows], dst_ref=tok_p.at[rows], send_sem=tsem.at[r], recv_sem=trec.at[r],
+            src_ref=tok_o.at[rows], dst_ref=tok_p.at[rows], send_sem=tsem.at[r], recv_sem=trec.at[r],
             device_id=peer, device_id_type=pl.DeviceIdType.MESH)
         cp.start()
         t_cp.append(cp)
+    c_kv2 = load2(wrk, wrv, oth, wkv, there, 384)
+    c_a2 = load2(wak, wav, oth, wa, there, 128)
+    c_q2 = load2(wrq, waq, oth, wq, there, 384)
+    c_small = [load(rgain, rgain_v), load(sink, sink_v)]
+    c_wo = [load(wre, wo.at[0, pl.ds(0, 384)]), load(wao, wo.at[1, pl.ds(0, 384)])]
+
+    def first_half(acc, w):
+        for r in range(2):
+            rows = pl.ds(r * HALF, HALF)
+            acc[rows] = dot(sc_o[rows], w[here])
+
+    def wait_all(cps):
+        for cp in cps:
+            cp.wait()
+
+    wait_all(c_kv)
+    first_half(acc_kv, wkv)
+    wait_all(c_a)
+    first_half(acc_a, wa)
+
+    inv = [None, None]
+    wait_all(c_kv2)
+    for r in range(2):
+        t_cp[r].wait_recv()
+
+        def peer_rows(i, carry):
+            r0 = pl.multiple_of(r * HALF + i * 64, 64)
+            s, part = scale_rows(tok_p, r0, g_p)
+            tok_p[pl.ds(r0, 64)] = s
+            total = jnp.sum(ssq[pl.ds(r0, 64)] + part, axis=1, keepdims=True)
+            ssq[pl.ds(r0, 64)] = jnp.broadcast_to(lax.rsqrt(total / D + EPS), (64, 128))
+            return carry
+
+        lax.fori_loop(0, HALF // 64, peer_rows, 0)
+        rows = pl.ds(r * HALF, HALF)
+        res = acc_kv[rows] + dot(tok_p[rows], wkv[there])
+        kv[rows] = (res * ssq[rows, 0:1]).astype(bf16)
+
     w_cp = []
     for i, w in enumerate((wre, wao)):
         cp = pltpu.make_async_remote_copy(
@@ -172,44 +214,6 @@
             device_id=peer, device_id_type=pl.DeviceIdType.MESH)
         cp.start()
         w_cp.append(cp)
-
-    c_kv2 = load2(wrk, wrv, oth, wkv, there, 384)
-    c_a2 = load2(wak, wav, oth, wa, there, 128)
-    c_q2 = load2(wrq, waq, oth, wq, there, 384)
-    c_small = [load(rgain, rgain_v), load(sink, sink_v)]
-    c_wo = [load(wre, wo.at[0, pl.ds(0, 384)]), load(wao, wo.at[1, pl.ds(0, 384)])]
-
-    def first_half(acc, w):
-        for r in range(2):
-            rows = pl.ds(r * HALF, HALF)
-            acc[rows] = dot(sc_o[rows], w[here])
-
-    def wait_all(cps):
-        for cp in cps:
-            cp.wait()
-
-    wait_all(c_kv)
-    first_half(acc_kv, wkv)
-    wait_all(c_a)
-    first_half(acc_a, wa)
-
-    inv = [None, None]
-    wait_all(c_kv2)
-    for r in range(2):
-        t_cp[r].wait_recv()
-
-        def peer_rows(i, carry):
-            r0 = pl.multiple_of(r * HALF + i * 64, 64)
-            s, part = scale_rows(tok_p, r0, g_p)
-            tok_p[pl.ds(r0, 64)] = s
-            total = jnp.sum(ssq[pl.ds(r0, 64)] + part, axis=1, keepdims=True)
-            ssq[pl.ds(r0, 64)] = jnp.broadcast_to(lax.rsqrt(total / D + EPS), (64, 128))
-            return carry
-
-        lax.fori_loop(0, HALF // 64, peer_rows, 0)
-        rows = pl.ds(r * HALF, HALF)
-        res = acc_kv[rows] + dot(tok_p[rows], wkv[there])
-        kv[rows] = (res * ssq[rows, 0:1]).astype(bf16)
 
     lo = iota((64, 128), 1) < 64
     s_p = [jnp.zeros((64, 128), f32) for _ in range(3)]
@@ -221,7 +225,7 @@
             tp_ = tot[:, p * 128:(p + 1) * 128]
             lcp = el[rows, cols]
             kd = (kv[rows, cols].astype(f32) * jnp.exp(tp_ - lcp)).astype(bf16)
-            m = t_dot(kd, kv[rows, pl.ds(384 + p * 128, 128)])
+            m = t_dot(kv[rows, pl.ds(384 + p * 128, 128)], kd)
             comp = jnp.where(lo, m[0:64], m[64:128])
             st[c, p] = s_p[p].astype(bf16)
             s_p[p] = jnp.exp(tp_) * s_p[p] + comp
@@ -276,26 +280,28 @@
     def spread(s):
         return jnp.concatenate([s * m0, s * m1], axis=0)
 
-    def ret_chunk(i, carry):
-        c = lax.rem(other * 3 + i, NC)
-        rows = pl.ds(pl.multiple_of(c * C, C), C)
-        past = et[pl.ds(c, 1)]
-        lrows = lcrow[pl.ds(pl.multiple_of(c * 8, 8), 8)]
-        for p in range(3):
-            cols = pl.ds(p * 128, 128)
-            q2, k2, v2 = qb[rows, cols], kv[rows, cols], kv[rows, pl.ds(384 + p * 128, 128)]
+    def ret_pair(i, carry):
+        todo = []
+        for u in range(2):
+            c = lax.rem(other * 3 + 2 * i + u, NC)
+            half, lanes = lax.div(c, 3), pl.ds(pl.multiple_of(lax.rem(c, 3) * C, C), C)
+            rows = pl.ds(pl.multiple_of(c * C, C), C)
+            eight = pl.ds(pl.multiple_of(c * 8, 8), 8)
+            for p in range(3):
+                q2 = qb[rows, pl.ds(p * 128, 128)]
+                s = dot_t(kv[rows, pl.ds(p * 128, 128)], jnp.concatenate([q2 * m0, q2 * m1], axis=0))
+                todo.append((p, half, lanes, rows, lcrow[eight], exr[eight], s, dot_t(spread(st[c, p]), q2)))
+        for p, half, lanes, rows, lrows, erows, s, past in todo:
             ws = []
-            for j, mj in enumerate((m0, m1)):
+            for j in range(2):
                 h = 2 * p + j
-                gap = lch[rows, pl.ds(h * 128, 128)] - lrows[h:h + 1] + biasc[...]
-                ws.append((dot_t(q2 * mj, k2) * jnp.exp(gap)).astype(bf16))
-            ex = jnp.exp(el[rows, cols])
-            el[rows, cols] = ex * past[:, p * 128:(p + 1) * 128]
-            ws.append((q2.astype(f32) * ex).astype(bf16))
-            rhs = jnp.concatenate([v2 * m0, v2 * m1, spread(st[c, p])], axis=0)
-            inner[rows, cols] = dot(jnp.concatenate(ws, axis=1), rhs)
+                gap = lrows[h:h + 1] - lch[rows, pl.ds(h * 128, 128)] + biasc[...]
+                ws.append((s[:, j * C:(j + 1) * C] * jnp.exp(gap)).astype(bf16))
+            o = t_dot(kv[rows, pl.ds(384 + p * 128, 128)], jnp.concatenate(ws, axis=1))
+            for j in range(2):
+                h, r = 2 * p + j, slice(j * 64, (j + 1) * 64)
+                inner[half, pl.ds(h * 64, 64), lanes] = o[r, j * C:(j + 1) * C] + past[r] * erows[h:h + 1]
         return carry
-
 
     for d in range(1, 4):
         arrived(st_a.at[0], buf_a.at[y_at[d]], asem.at[d - 1], arec.at[y_at[d]], at_y(d))
@@ -316,43 +322,58 @@
     buf_b[z] = g_b[...]
     buf_bl[z] = l_b[...]
 
+    lax.fori_loop(0, 2, ret_pair, 0)
+
     wait_all(c_small)
     halo.wait_recv()
+    for p in range(3):
+        g = jnp.broadcast_to(rgain_v[pl.ds(p * C, C)].reshape(1, C), (C, C))
+        gcol[pl.ds(p * C, C)] = jnp.transpose(g)
     sink_row = jnp.concatenate(
         [jnp.broadcast_to(sink_v[0:1, h:h + 1], (1, C)) for h in range(6)], axis=1)
 
-    def att_block(i, half):
-        n = half * 3 + i
-        bandr = pl.ds(pl.multiple_of(n * C, C), 2 * C)
-        edge = (n == 0) & (sp == 0)
-        s = dot_t(akv[bandr, pl.ds(0, 128)], qs[n])
+    def att_half(half):
         is_own = iota((C, C), 0) <= iota((C, C), 1)
-        ws, scale = [], []
-        for h in range(6):
-            hc = slice(h * C, (h + 1) * C)
-            past = jnp.where(edge, NEG, s[:C, hc])
-            v = jnp.where(is_own, s[C:, hc], past)
-            sk = sink_row[:, hc]
-            top = jnp.maximum(jnp.max(v, axis=0, keepdims=True), sk)
-            e = jnp.exp(v - top)
-            scale.append(1.0 / (jnp.sum(e, axis=0, keepdims=True) + jnp.exp(sk - top)))
-            eb = e.astype(bf16)
-            ws.append(jnp.concatenate([eb * wmask[0:C], eb * wmask[C:]], axis=0))
-        o = t_dot(akv[bandr, pl.ds(128, 128)], jnp.concatenate(ws, axis=1))
-        cols = pl.ds(pl.multiple_of(i * C, C), C)
-        for h in range(6):
-            r0 = 64 if h >= 3 else 0
-            att[half, pl.ds(h * 64, 64), cols] = (
-                o[r0:r0 + 64, h * C:(h + 1) * C] * scale[h]).astype(bf16)
-        return half
+
+        def scores(i):
+            n = half * 3 + i
+            return dot_t(akv[pl.ds(pl.multiple_of(n * C, C), 2 * C), pl.ds(0, 128)], qs[n])
+
+        def block(i, s):
+            n = half * 3 + i
+            ws, scale = [], []
+            for h in range(6):
+                hc = slice(h * C, (h + 1) * C)
+                past = s[:C, hc]
+                if i == 0:
+                    past = jnp.where((n == 0) & (sp == 0), NEG, past)
+                v = jnp.where(is_own, s[C:, hc], past)
+                sk = sink_row[:, hc]
+                top = jnp.maximum(jnp.max(v, axis=0, keepdims=True), sk)
+                e = jnp.exp(v - top)
+                scale.append(1.0 / (jnp.sum(e, axis=0, keepdims=True) + jnp.exp(sk - top)))
+                eb = e.astype(bf16)
+                ws.append(jnp.concatenate([eb * wmask[0:C], eb * wmask[C:]], axis=0))
+            bandr = pl.ds(pl.multiple_of(n * C, C), 2 * C)
+            return scale, t_dot(akv[bandr, pl.ds(128, 128)], jnp.concatenate(ws, axis=1))
+
+        ahead = scores(0)
+        for i in range(3):
+            s = ahead
+            if i < 2:
+                ahead = scores(i + 1)
+            scale, o = block(i, s)
+            for h in range(6):
+                r0 = 64 if h >= 3 else 0
+                att[half, pl.ds(h * 64, 64), pl.ds(i * C, C)] = (
+                    o[r0:r0 + 64, h * C:(h + 1) * C] * scale[h]).astype(bf16)
 
     mine = pl.ds(pl.multiple_of(tp * HALF, HALF), HALF)
     theirs = pl.ds(pl.multiple_of(other * HALF, HALF), HALF)
     o_cp = []
-    lax.fori_loop(0, 3, att_block, other)
+    att_half(other)
     send(att.at[other], att_p, osem.at[0], orec.at[0], peer, o_cp)
-    lax.fori_loop(0, 3, att_block, tp)
-    lax.fori_loop(0, 4, ret_chunk, 0)
+    att_half(tp)
 
     for d in range(1, 8):
         arrived(g_b, buf_b.at[z_at[d]], bsem.at[d - 1], brec.at[z_at[d]], at_z(d))
@@ -370,7 +391,7 @@
         send(s_c.at[y_at[d]], buf_c.at[y], csem.at[d - 1], crec.at[y], at_y(d), c_cp)
     buf_c[y] = s_c[y]
 
-    lax.fori_loop(4, NC, ret_chunk, 0)
+    ret_pair(2, 0)
 
     wait_all(c_wo)
     w_cp[0].wait_recv()
@@ -384,26 +405,30 @@
     for d in range(1, 4):
         arrived(s_c.at[0], buf_c.at[y_at[d]], csem.at[d - 1], crec.at[y_at[d]], at_y(d))
     big = [spread(jnp.concatenate([buf_c[q, p] for q in range(4)], axis=0)) for p in range(3)]
-    ones_bd = jnp.where(
-        lax.div(iota((128, 128), 0), 64) == lax.div(iota((128, 128), 1), 64), 1.0, 0.0).astype(bf16)
-
-    def finish(rows):
+
+    def finish(hf, rows):
         for p in range(3):
-            cols = pl.ds(p * 128, 128)
-            full = inner[rows, cols] + dot(qb[rows, cols], big[p]) * el[rows, cols]
-            ms = dot((full * full).astype(bf16), ones_bd) * (1.0 / 64)
-            ret[rows, cols] = (full * lax.rsqrt(ms + EPS) * rgain_v[cols].reshape(1, 128)).astype(bf16)
-
-    finish(theirs)
-    send(ret.at[theirs], ret_p, osem.at[1], orec.at[1], peer, o_cp)
-    finish(mine)
+            car = dot_t(big[p], qb[rows, pl.ds(p * 128, 128)])
+            for b in range(3):
+                lanes = slice(b * C, (b + 1) * C)
+                f8 = frow[pl.ds(pl.multiple_of((hf * 3 + b) * 8, 8), 8)]
+                for j in range(2):
+                    h = 2 * p + j
+                    hr = pl.ds(h * 64, 64)
+                    full = inner[hf, hr, pl.ds(b * C, C)] + car[j * 64:(j + 1) * 64, lanes] * f8[h:h + 1]
+                    ms = jnp.sum(full * full, axis=0, keepdims=True) * (1.0 / 64)
+                    ret[hf, hr, pl.ds(b * C, C)] = (full * lax.rsqrt(ms + EPS) * gcol[hr]).astype(bf16)
+
+    finish(other, theirs)
+    send(ret.at[other], ret_p, osem.at[1], orec.at[1], peer, o_cp)
+    finish(tp, mine)
     for j in range(4):
         cols = pl.ds(j * 512, 512)
-        oacc[:, cols] += dot(ret[mine], wo[0, 0:384, cols])
+        oacc[:, cols] += t_dot(ret[tp], wo[0, 0:384, cols])
     o_cp[1].wait_recv()
     for j in range(4):
         cols = pl.ds(j * 512, 512)
-        out[0, :, cols] = (oacc[:, cols] + dot(ret_p[...], wo[0, 384:768, cols])).astype(bf16)
+        out[0, :, cols] = (oacc[:, cols] + t_dot(ret_p[...], wo[0, 384:768, cols])).astype(bf16)
 
     for cp in t_cp + w_cp + a_cp + al_cp + b_cp + bl_cp + c_cp + o_cp + [halo]:
         cp.wait_send()
@@ -420,14 +445,14 @@
         V((D, 768), bf16), V((D, 768), bf16), V((D, 256), bf16),
         V((T, 768), f32), V((T, 256), f32),
         V((T, 768), bf16), V((T, 384), bf16), V((T + C, 256), bf16), V((NC, 768, 128), bf16),
-        V((48, 128), f32), V((T, 768), f32), V((T, 384), f32), V((8, 384), f32), V((8, 384), f32),
-        V((NC, 3, 64, 128), bf16), V((T, 384), f32),
+        V((48, 128), f32), V((48, 128), f32), V((48, 128), f32), V((T, 768), f32), V((T, 384), f32), V((8, 384), f32),
+        V((NC, 3, 64, 128), bf16), V((2, 384, HALF), f32), V((384, 128), f32),
         V((2 * C, C), bf16), V((C, C), f32),
         V((4, 3, 16, 128), bf16), V((4, 3, 16, 128), bf16), V((8, 128), f32), V((4, 8, 128), f32),
         V((3, 16, 128), bf16), V((8, 3, 16, 128), bf16), V((8, 128), f32), V((8, 8, 128), f32),
         V((4, 3, 16, 128), bf16), V((4, 3, 16, 128), bf16),
-        V((2, 768, D), bf16), V((2, 384, HALF), bf16), V((384, HALF), bf16), V((T, 384), bf16),
-        V((HALF, 384), bf16), V((HALF, D), f32),
+        V((2, 768, D), bf16), V((2, 384, HALF), bf16), V((384, HALF), bf16), V((2, 384, HALF), bf16),
+        V((384, HALF), bf16), V((HALF, D), f32),
         DMA((24,)), DMA((2,)), DMA((2,)), DMA((2,)), DMA((2,)), DMA(()), DMA(()),
         DMA((3,)), DMA((4,)), DMA((3,)), DMA((4,)), DMA((7,)), DMA((8,)), DMA((7,)), DMA((8,)),
         DMA((3,)), DMA((4,)), DMA((2,)), DMA((2,)),

time: 34.7 us -> 33.4 us (0.963)
  Pallas kernels: 33.4 us -> 32.1 us
    pallas_call x1, Pallas kernels: 33.4 us -> 32.1 us  [shards(): pl.pallas_call(kernel, out_shape=jax.ShapeDtypeStruct((1, HALF, D), bf16)...]
where the time goes in v3:
time: 33.4 us; the launch traced here: 33.3 us
  Pallas kernels  32.1 us (96%)
  local copies, waits for them, and re-layouts  1.15 us (3%)
    pallas_call x1, Pallas kernels, shards(): pl.pallas_call(kernel, out_shape=jax.ShapeDtypeStruct((1, HALF, D), bf16)...  32.1 us
    unnamed x1, local copies, waits for them, and re-layouts  1.15 us

profile of v3, /device:TPU:1, one launch (start us, length us, event | category | flops | bytes accessed | tf_op | source)
XLA Modules:
  0.0 33.3 jit_solution(3042495944833063318)
XLA Ops:
  0.0 32.1 %shard_map.127 = bf16[1,384,2048]{2,1,0:T(8,128)(2,1)S(1)} custom-call(bf16[1,768,1024]{2,1,0:T(8,128)(2,1)} %tok.1, f32[1,2048]{1,0:T(1,128)} %bitcast.4, bf16[2048,384]{1,0:T(8,128)(2,1)} %wrq.1, bf16[2048,384]{1,0:T(8,128)(2,1)} %wrk.1, bf16[2048,384]{1,0:T(8,128)(2,1)} %wrv.1, bf16[2048,384]{1,0:T(8,128)(2,1)} %waq.1, bf16[2048,128]{1,0:T(8,128)(2,1)} %wak.1, ...), custom_call_target="tpu_custom_call" | custom-call | tf_op jit(solution)/shard_map/pallas_call | solution.py:460
  32.1 1.1 %copy.15 = bf16[1,384,2048]{2,1,0:T(8,128)(2,1)} copy(bf16[1,384,2048]{2,1,0:T(8,128)(2,1)S(1)} %shard_map.127) | data formatting | bytes 3145728

commit v4 on v3

--- a/solution.py
+++ b/solution.py
@@ -131,6 +131,7 @@
         lc8 = lc[c * 8:(c + 1) * 8]
         frow[c * 8:(c + 1) * 8] = jnp.exp(lc8 + before8)
         before8 = before8 + lc8[:, C - 1:C]
+    l_a[...] = jnp.zeros((8, 128), f32)
     for p in range(3):
         l_a[p:p + 1] = before[:, p * 128:(p + 1) * 128]
 
@@ -138,7 +139,10 @@
     c_tok.wait()
     c_kv = load2(wrk, wrv, own, wkv, here, 384)
     c_a = load2(wak, wav, own, wa, here, 128)
+    c_kv2 = load2(wrk, wrv, oth, wkv, there, 384)
+    c_a2 = load2(wak, wav, oth, wa, there, 128)
     c_q = load2(wrq, waq, own, wq, here, 384)
+    c_q2 = load2(wrq, waq, oth, wq, there, 384)
     g_o = gain_v[:, own]
     g_p = gain_v[:, oth]
 
@@ -169,11 +173,23 @@
             device_id=peer, device_id_type=pl.DeviceIdType.MESH)
         cp.start()
         t_cp.append(cp)
-    c_kv2 = load2(wrk, wrv, oth, wkv, there, 384)
-    c_a2 = load2(wak, wav, oth, wa, there, 128)
-    c_q2 = load2(wrq, waq, oth, wq, there, 384)
-    c_small = [load(rgain, rgain_v), load(sink, sink_v)]
-    c_wo = [load(wre, wo.at[0, pl.ds(0, 384)]), load(wao, wo.at[1, pl.ds(0, 384)])]
+    a_cp, al_cp, b_cp, bl_cp = [], [], [], []
+
+    def send(src, dst, ss, rs, who, group):
+        cp = pltpu.make_async_remote_copy(
+            src_ref=src, dst_ref=dst, send_sem=ss, recv_sem=rs, device_id=who,
+            device_id_type=pl.DeviceIdType.MESH)
+        cp.start()
+        group.append(cp)
+
+    def arrived(src, dst, ss, rs, who):
+        pltpu.make_async_remote_copy(
+            src_ref=src, dst_ref=dst, send_sem=ss, recv_sem=rs, device_id=who,
+            device_id_type=pl.DeviceIdType.MESH).wait_recv()
+
+    for d in range(1, 4):
+        send(l_a, buf_al.at[y], alsem.at[d - 1], alrec.at[y], at_y(d), al_cp)
+    buf_al[y] = l_a[...]
 
     def first_half(acc, w):
         for r in range(2):
@@ -189,7 +205,9 @@
     wait_all(c_a)
     first_half(acc_a, wa)
 
-    inv = [None, None]
+    c_small = [load(rgain, rgain_v), load(sink, sink_v)]
+    c_wo = [load(wre, wo.at[0, pl.ds(0, 384)]), load(wao, wo.at[1, pl.ds(0, 384)])]
+
     wait_all(c_kv2)
     for r in range(2):
         t_cp[r].wait_recv()
@@ -207,13 +225,12 @@
         res = acc_kv[rows] + dot(tok_p[rows], wkv[there])
         kv[rows] = (res * ssq[rows, 0:1]).astype(bf16)
 
-    w_cp = []
-    for i, w in enumerate((wre, wao)):
-        cp = pltpu.make_async_remote_copy(
-            src_ref=w, dst_ref=wo.at[i, pl.ds(384, 384)], send_sem=wsem.at[i], recv_sem=wrec.at[i],
-            device_id=peer, device_id_type=pl.DeviceIdType.MESH)
-        cp.start()
-        w_cp.append(cp)
+    for d in range(1, 4):
+        arrived(l_a, buf_al.at[y_at[d]], alsem.at[d - 1], alrec.at[y_at[d]], at_y(d))
+    l_b[...] = buf_al[0] + buf_al[1] + buf_al[2] + buf_al[3]
+    for d in range(1, 8):
+        send(l_b, buf_bl.at[z], blsem.at[d - 1], blrec.at[z], at_z(d), bl_cp)
+    buf_bl[z] = l_b[...]
 
     lo = iota((64, 128), 1) < 64
     s_p = [jnp.zeros((64, 128), f32) for _ in range(3)]
@@ -233,25 +250,17 @@
         for q in range(4):
             st_a[q, p] = s_p[p][q * 16:(q + 1) * 16].astype(bf16)
 
-    a_cp, al_cp = [], []
-
-    def send(src, dst, ss, rs, who, group):
+    for d in range(1, 4):
+        send(st_a.at[y_at[d]], buf_a.at[y], asem.at[d - 1], arec.at[y], at_y(d), a_cp)
+    buf_a[y] = st_a[y]
+
+    w_cp = []
+    for i, w in enumerate((wre, wao)):
         cp = pltpu.make_async_remote_copy(
-            src_ref=src, dst_ref=dst, send_sem=ss, recv_sem=rs, device_id=who,
-            device_id_type=pl.DeviceIdType.MESH)
+            src_ref=w, dst_ref=wo.at[i, pl.ds(384, 384)], send_sem=wsem.at[i], recv_sem=wrec.at[i],
+            device_id=peer, device_id_type=pl.DeviceIdType.MESH)
         cp.start()
-        group.append(cp)
-
-    def arrived(src, dst, ss, rs, who):
-        pltpu.make_async_remote_copy(
-            src_ref=src, dst_ref=dst, send_sem=ss, recv_sem=rs, device_id=who,
-            device_id_type=pl.DeviceIdType.MESH).wait_recv()
-
-    for d in range(1, 4):
-        send(st_a.at[y_at[d]], buf_a.at[y], asem.at[d - 1], arec.at[y], at_y(d), a_cp)
-        send(l_a, buf_al.at[y], alsem.at[d - 1], alrec.at[y], at_y(d), al_cp)
-    buf_a[y] = st_a[y]
-    buf_al[y] = l_a[...]
+        w_cp.append(cp)
 
     wait_all(c_a2)
     for r in range(2):
@@ -305,22 +314,15 @@
 
     for d in range(1, 4):
         arrived(st_a.at[0], buf_a.at[y_at[d]], asem.at[d - 1], arec.at[y_at[d]], at_y(d))
-        arrived(l_a, buf_al.at[y_at[d]], alsem.at[d - 1], alrec.at[y_at[d]], at_y(d))
-    b_cp, bl_cp = [], []
     for p in range(3):
         e = jnp.zeros((16, 128), f32)
-        ltot = jnp.zeros((1, 128), f32)
         for yy in range(4):
             lyy = buf_al[yy][p:p + 1]
             e = jnp.exp(lyy) * e + buf_a[yy, p].astype(f32)
-            ltot = ltot + lyy
         g_b[p] = e.astype(bf16)
-        l_b[p:p + 1] = ltot
     for d in range(1, 8):
         send(g_b, buf_b.at[z], bsem.at[d - 1], brec.at[z], at_z(d), b_cp)
-        send(l_b, buf_bl.at[z], blsem.at[d - 1], blrec.at[z], at_z(d), bl_cp)
     buf_b[z] = g_b[...]
-    buf_bl[z] = l_b[...]
 
     lax.fori_loop(0, 2, ret_pair, 0)
 

time: 33.4 us -> 32.9 us (0.985)
  Pallas kernels: 32.1 us -> 31.6 us
    pallas_call x1, Pallas kernels: 32.1 us -> 31.6 us  [shards(): pl.pallas_call(kernel, out_shape=jax.ShapeDtypeStruct((1, HALF, D), bf16)...]
where the time goes in v4:
time: 32.9 us; the launch traced here: 32.8 us
  Pallas kernels  31.6 us (96%)
  local copies, waits for them, and re-layouts  1.15 us (3%)
    pallas_call x1, Pallas kernels, shards(): pl.pallas_call(kernel, out_shape=jax.ShapeDtypeStruct((1, HALF, D), bf16)...  31.6 us
    unnamed x1, local copies, waits for them, and re-layouts  1.15 us

profile of v4, /device:TPU:1, one launch (start us, length us, event | category | flops | bytes accessed | tf_op | source)
XLA Modules:
  0.0 32.8 jit_solution(797005233406234429)
XLA Ops:
  0.0 31.6 %shard_map.127 = bf16[1,384,2048]{2,1,0:T(8,128)(2,1)S(1)} custom-call(bf16[1,768,1024]{2,1,0:T(8,128)(2,1)} %tok.1, f32[1,2048]{1,0:T(1,128)} %bitcast.4, bf16[2048,384]{1,0:T(8,128)(2,1)} %wrq.1, bf16[2048,384]{1,0:T(8,128)(2,1)} %wrk.1, bf16[2048,384]{1,0:T(8,128)(2,1)} %wrv.1, bf16[2048,384]{1,0:T(8,128)(2,1)} %waq.1, bf16[2048,128]{1,0:T(8,128)(2,1)} %wak.1, ...), custom_call_target="tpu_custom_call" | custom-call | tf_op jit(solution)/shard_map/pallas_call | solution.py:462
  31.6 1.1 %copy.15 = bf16[1,384,2048]{2,1,0:T(8,128)(2,1)} copy(bf16[1,384,2048]{2,1,0:T(8,128)(2,1)S(1)} %shard_map.127) | data formatting | bytes 3145728

commit v5 on v4

--- a/solution.py
+++ b/solution.py
@@ -51,9 +51,9 @@
     lcrow, exr, frow, lch, el, tots, st, inner, gcol,
     wmask, biasc,
     st_a, buf_a, l_a, buf_al, g_b, buf_b, l_b, buf_bl, s_c, buf_c,
-    wo, att, att_p, ret, ret_p, oacc,
+    wo, att, att_p, ret, oacc, in_p, q_p, frow_p, gcol_p,
     lsem, tsem, trec, wsem, wrec, hsem, hrec,
-    asem, arec, alsem, alrec, bsem, brec, blsem, blrec, csem, crec, osem, orec,
+    asem, arec, alsem, alrec, bsem, brec, blsem, blrec, csem, crec, osem, orec, xsem, xrec,
 ):
     sp = lax.axis_index("sp")
     tp = lax.axis_index("tp")
@@ -70,11 +70,14 @@
     def at_z(d):
         return {"sp": z_at[d] * 4 + y}
 
+    def across_y(d):
+        return {"sp": z * 4 + y_at[d], "tp": other}
+
     nxt = {"sp": lax.rem(sp + 1, 32)}
     prv = {"sp": lax.rem(sp + 31, 32)}
 
     barrier = pltpu.get_barrier_semaphore()
-    greet = [peer] + [at_y(d) for d in range(1, 4)] + [at_z(d) for d in range(1, 8)] + [prv]
+    greet = [peer] + [at_y(d) for d in range(1, 4)] + [across_y(d) for d in range(1, 4)] + [at_z(d) for d in range(1, 8)] + [prv]
     for who in greet:
         pl.semaphore_signal(barrier, inc=1, device_id=who, device_id_type=pl.DeviceIdType.MESH)
 
@@ -190,6 +193,8 @@
     for d in range(1, 4):
         send(l_a, buf_al.at[y], alsem.at[d - 1], alrec.at[y], at_y(d), al_cp)
     buf_al[y] = l_a[...]
+    x_cp = []
+    send(frow, frow_p, xsem.at[0], xrec.at[0], peer, x_cp)
 
     def first_half(acc, w):
         for r in range(2):
@@ -312,6 +317,9 @@
                 inner[half, pl.ds(h * 64, 64), lanes] = o[r, j * C:(j + 1) * C] + past[r] * erows[h:h + 1]
         return carry
 
+    mine = pl.ds(pl.multiple_of(tp * HALF, HALF), HALF)
+    theirs = pl.ds(pl.multiple_of(other * HALF, HALF), HALF)
+
     for d in range(1, 4):
         arrived(st_a.at[0], buf_a.at[y_at[d]], asem.at[d - 1], arec.at[y_at[d]], at_y(d))
     for p in range(3):
@@ -324,6 +332,7 @@
         send(g_b, buf_b.at[z], bsem.at[d - 1], brec.at[z], at_z(d), b_cp)
     buf_b[z] = g_b[...]
 
+    send(qb.at[theirs], q_p, xsem.at[1], xrec.at[1], peer, x_cp)
     lax.fori_loop(0, 2, ret_pair, 0)
 
     wait_all(c_small)
@@ -370,10 +379,10 @@
                 att[half, pl.ds(h * 64, 64), pl.ds(i * C, C)] = (
                     o[r0:r0 + 64, h * C:(h + 1) * C] * scale[h]).astype(bf16)
 
-    mine = pl.ds(pl.multiple_of(tp * HALF, HALF), HALF)
-    theirs = pl.ds(pl.multiple_of(other * HALF, HALF), HALF)
     o_cp = []
     att_half(other)
+    send(inner.at[other], in_p, xsem.at[2], xrec.at[2], peer, x_cp)
+    send(gcol, gcol_p, xsem.at[3], xrec.at[3], peer, x_cp)
     send(att.at[other], att_p, osem.at[0], orec.at[0], peer, o_cp)
     att_half(tp)
 
@@ -390,8 +399,10 @@
             e = jnp.exp(buf_al[yy][p:p + 1]) * e + buf_a[yy, p].astype(f32)
     c_cp = []
     for d in range(1, 4):
-        send(s_c.at[y_at[d]], buf_c.at[y], csem.at[d - 1], crec.at[y], at_y(d), c_cp)
-    buf_c[y] = s_c[y]
+        send(s_c.at[y_at[d]], buf_c.at[0, y], csem.at[d - 1], crec.at[0, y], at_y(d), c_cp)
+        send(s_c.at[y_at[d]], buf_c.at[1, y], csem.at[d + 2], crec.at[1, y], across_y(d), c_cp)
+    send(s_c.at[y], buf_c.at[1, y], csem.at[6], crec.at[1, y], peer, c_cp)
+    buf_c[0, y] = s_c[y]
 
     ret_pair(2, 0)
 
@@ -404,35 +415,32 @@
         cols = pl.ds(j * 512, 512)
         oacc[:, cols] = t_dot(lhs, wo[1, :, cols])
 
-    for d in range(1, 4):
-        arrived(s_c.at[0], buf_c.at[y_at[d]], csem.at[d - 1], crec.at[y_at[d]], at_y(d))
-    big = [spread(jnp.concatenate([buf_c[q, p] for q in range(4)], axis=0)) for p in range(3)]
-
-    def finish(hf, rows):
+    for cp in x_cp:
+        cp.wait_recv()
+    for d in range(1, 4):
+        arrived(s_c.at[0], buf_c.at[0, y_at[d]], csem.at[0], crec.at[0, y_at[d]], at_y(d))
+    for d in range(4):
+        arrived(s_c.at[0], buf_c.at[1, y_at[d]], csem.at[0], crec.at[1, y_at[d]], peer)
+    sides = ((inner.at[tp], qb.at[mine], frow, gcol), (in_p, q_p, frow_p, gcol_p))
+    for side, (inn, qrows, factors, gains) in enumerate(sides):
         for p in range(3):
-            car = dot_t(big[p], qb[rows, pl.ds(p * 128, 128)])
+            big = spread(jnp.concatenate([buf_c[side, q, p] for q in range(4)], axis=0))
+            car = dot_t(big, qrows[:, p * 128:(p + 1) * 128])
             for b in range(3):
                 lanes = slice(b * C, (b + 1) * C)
-                f8 = frow[pl.ds(pl.multiple_of((hf * 3 + b) * 8, 8), 8)]
+                f8 = factors[pl.ds(pl.multiple_of((tp * 3 + b) * 8, 8), 8)]
                 for j in range(2):
                     h = 2 * p + j
-                    hr = pl.ds(h * 64, 64)
-                    full = inner[hf, hr, pl.ds(b * C, C)] + car[j * 64:(j + 1) * 64, lanes] * f8[h:h + 1]
+                    hr = slice(h * 64, (h + 1) * 64)
+                    full = inn[hr, lanes] + car[j * 64:(j + 1) * 64, lanes] * f8[h:h + 1]
                     ms = jnp.sum(full * full, axis=0, keepdims=True) * (1.0 / 64)
-                    ret[hf, hr, pl.ds(b * C, C)] = (full * lax.rsqrt(ms + EPS) * gcol[hr]).astype(bf16)
-
-    finish(other, theirs)
-    send(ret.at[other], ret_p, osem.at[1], orec.at[1], peer, o_cp)
-    finish(tp, mine)
-    for j in range(4):
-        cols = pl.ds(j * 512, 512)
-        oacc[:, cols] += t_dot(ret[tp], wo[0, 0:384, cols])
-    o_cp[1].wait_recv()
-    for j in range(4):
-        cols = pl.ds(j * 512, 512)
-        out[0, :, cols] = (oacc[:, cols] + t_dot(ret_p[...], wo[0, 384:768, cols])).astype(bf16)
-
-    for cp in t_cp + w_cp + a_cp + al_cp + b_cp + bl_cp + c_cp + o_cp + [halo]:
+                    ret[side * 384 + h * 64:side * 384 + (h + 1) * 64, lanes] = (
+                        full * lax.rsqrt(ms + EPS) * gains[hr]).astype(bf16)
+    for j in range(2):
+        cols = pl.ds(j * 1024, 1024)
+        out[0, :, cols] = (oacc[:, cols] + t_dot(ret[...], wo[0, :, cols])).astype(bf16)
+
+    for cp in t_cp + w_cp + a_cp + al_cp + b_cp + bl_cp + c_cp + o_cp + x_cp + [halo]:
         cp.wait_send()
 
 
@@ -452,12 +460,12 @@
         V((2 * C, C), bf16), V((C, C), f32),
         V((4, 3, 16, 128), bf16), V((4, 3, 16, 128), bf16), V((8, 128), f32), V((4, 8, 128), f32),
         V((3, 16, 128), bf16), V((8, 3, 16, 128), bf16), V((8, 128), f32), V((8, 8, 128), f32),
-        V((4, 3, 16, 128), bf16), V((4, 3, 16, 128), bf16),
-        V((2, 768, D), bf16), V((2, 384, HALF), bf16), V((384, HALF), bf16), V((2, 384, HALF), bf16),
-        V((384, HALF), bf16), V((HALF, D), f32),
+        V((4, 3, 16, 128), bf16), V((2, 4, 3, 16, 128), bf16),
+        V((2, 768, D), bf16), V((2, 384, HALF), bf16), V((384, HALF), bf16), V((768, HALF), bf16),
+        V((HALF, D), f32), V((384, HALF), f32), V((HALF, 384), bf16), V((48, 128), f32), V((384, 128), f32),
         DMA((24,)), DMA((2,)), DMA((2,)), DMA((2,)), DMA((2,)), DMA(()), DMA(()),
         DMA((3,)), DMA((4,)), DMA((3,)), DMA((4,)), DMA((7,)), DMA((8,)), DMA((7,)), DMA((8,)),
-        DMA((3,)), DMA((4,)), DMA((2,)), DMA((2,)),
+        DMA((7,)), DMA((2, 4)), DMA((1,)), DMA((1,)), DMA((4,)), DMA((4,)),
     ]
     return pl.pallas_call(
         kernel,

time: 32.9 us -> 32.4 us (0.985)
  Pallas kernels: 31.6 us -> 31.2 us
    pallas_call x1, Pallas kernels: 31.6 us -> 31.2 us  [shards(): pl.pallas_call(kernel, out_shape=jax.ShapeDtypeStruct((1, HALF, D), bf16)...]
where the time goes in v5:
time: 32.4 us; the launch traced here: 32.3 us
  Pallas kernels  31.2 us (96%)
  local copies, waits for them, and re-layouts  1.15 us (4%)
    pallas_call x1, Pallas kernels, shards(): pl.pallas_call(kernel, out_shape=jax.ShapeDtypeStruct((1, HALF, D), bf16)...  31.2 us
    unnamed x1, local copies, waits for them, and re-layouts  1.15 us

profile of v5, /device:TPU:1, one launch (start us, length us, event | category | flops | bytes accessed | tf_op | source)
XLA Modules:
  0.0 32.3 jit_solution(347068484349506109)
XLA Ops:
  0.0 31.2 %shard_map.127 = bf16[1,384,2048]{2,1,0:T(8,128)(2,1)S(1)} custom-call(bf16[1,768,1024]{2,1,0:T(8,128)(2,1)} %tok.1, f32[1,2048]{1,0:T(1,128)} %bitcast.4, bf16[2048,384]{1,0:T(8,128)(2,1)} %wrq.1, bf16[2048,384]{1,0:T(8,128)(2,1)} %wrk.1, bf16[2048,384]{1,0:T(8,128)(2,1)} %wrv.1, bf16[2048,384]{1,0:T(8,128)(2,1)} %waq.1, bf16[2048,128]{1,0:T(8,128)(2,1)} %wak.1, ...), custom_call_target="tpu_custom_call" | custom-call | tf_op jit(solution)/shard_map/pallas_call | solution.py:470
  31.2 1.1 %copy.15 = bf16[1,384,2048]{2,1,0:T(8,128)(2,1)} copy(bf16[1,384,2048]{2,1,0:T(8,128)(2,1)S(1)} %shard_map.127) | data formatting | bytes 3145728

commit v6 on v5

--- a/solution.py
+++ b/solution.py
@@ -13,6 +13,8 @@
 HALF = 384
 C = 128
 NC = 6
+YS = (2, 1, 3)
+ZS = (4, 3, 5, 2, 6, 1, 7)
 NEG = float("-inf")
 f32 = jnp.float32
 bf16 = jnp.bfloat16
@@ -77,7 +79,7 @@
     prv = {"sp": lax.rem(sp + 31, 32)}
 
     barrier = pltpu.get_barrier_semaphore()
-    greet = [peer] + [at_y(d) for d in range(1, 4)] + [across_y(d) for d in range(1, 4)] + [at_z(d) for d in range(1, 8)] + [prv]
+    greet = [at_z(d) for d in ZS] + [at_y(d) for d in YS] + [across_y(d) for d in YS] + [prv, peer]
     for who in greet:
         pl.semaphore_signal(barrier, inc=1, device_id=who, device_id_type=pl.DeviceIdType.MESH)
 
@@ -190,7 +192,7 @@
             src_ref=src, dst_ref=dst, send_sem=ss, recv_sem=rs, device_id=who,
             device_id_type=pl.DeviceIdType.MESH).wait_recv()
 
-    for d in range(1, 4):
+    for d in YS:
         send(l_a, buf_al.at[y], alsem.at[d - 1], alrec.at[y], at_y(d), al_cp)
     buf_al[y] = l_a[...]
     x_cp = []
@@ -233,7 +235,7 @@
     for d in range(1, 4):
         arrived(l_a, buf_al.at[y_at[d]], alsem.at[d - 1], alrec.at[y_at[d]], at_y(d))
     l_b[...] = buf_al[0] + buf_al[1] + buf_al[2] + buf_al[3]
-    for d in range(1, 8):
+    for d in ZS:
         send(l_b, buf_bl.at[z], blsem.at[d - 1], blrec.at[z], at_z(d), bl_cp)
     buf_bl[z] = l_b[...]
 
@@ -255,7 +257,7 @@
         for q in range(4):
             st_a[q, p] = s_p[p][q * 16:(q + 1) * 16].astype(bf16)
 
-    for d in range(1, 4):
+    for d in YS:
         send(st_a.at[y_at[d]], buf_a.at[y], asem.at[d - 1], arec.at[y], at_y(d), a_cp)
     buf_a[y] = st_a[y]
 
@@ -328,7 +330,7 @@
             lyy = buf_al[yy][p:p + 1]
             e = jnp.exp(lyy) * e + buf_a[yy, p].astype(f32)
         g_b[p] = e.astype(bf16)
-    for d in range(1, 8):
+    for d in ZS:
         send(g_b, buf_b.at[z], bsem.at[d - 1], brec.at[z], at_z(d), b_cp)
     buf_b[z] = g_b[...]
 
@@ -398,7 +400,7 @@
             s_c[yy, p] = e.astype(bf16)
             e = jnp.exp(buf_al[yy][p:p + 1]) * e + buf_a[yy, p].astype(f32)
     c_cp = []
-    for d in range(1, 4):
+    for d in YS:
         send(s_c.at[y_at[d]], buf_c.at[0, y], csem.at[d - 1], crec.at[0, y], at_y(d), c_cp)
         send(s_c.at[y_at[d]], buf_c.at[1, y], csem.at[d + 2], crec.at[1, y], across_y(d), c_cp)
     send(s_c.at[y], buf_c.at[1, y], csem.at[6], crec.at[1, y], peer, c_cp)

time: 32.4 us -> 31.7 us (0.978)
  Pallas kernels: 31.2 us -> 30.5 us
    pallas_call x1, Pallas kernels: 31.2 us -> 30.5 us  [shards(): pl.pallas_call(kernel, out_shape=jax.ShapeDtypeStruct((1, HALF, D), bf16)...]
where the time goes in v6:
time: 31.7 us; the launch traced here: 31.6 us
  Pallas kernels  30.5 us (96%)
  local copies, waits for them, and re-layouts  1.15 us (4%)
    pallas_call x1, Pallas kernels, shards(): pl.pallas_call(kernel, out_shape=jax.ShapeDtypeStruct((1, HALF, D), bf16)...  30.5 us
    unnamed x1, local copies, waits for them, and re-layouts  1.15 us

profile of v6, /device:TPU:1, one launch (start us, length us, event | category | flops | bytes accessed | tf_op | source)
XLA Modules:
  0.0 31.6 jit_solution(5273974234835494871)
XLA Ops:
  0.0 30.5 %shard_map.127 = bf16[1,384,2048]{2,1,0:T(8,128)(2,1)S(1)} custom-call(bf16[1,768,1024]{2,1,0:T(8,128)(2,1)} %tok.1, f32[1,2048]{1,0:T(1,128)} %bitcast.4, bf16[2048,384]{1,0:T(8,128)(2,1)} %wrq.1, bf16[2048,384]{1,0:T(8,128)(2,1)} %wrk.1, bf16[2048,384]{1,0:T(8,128)(2,1)} %wrv.1, bf16[2048,384]{1,0:T(8,128)(2,1)} %waq.1, bf16[2048,128]{1,0:T(8,128)(2,1)} %wak.1, ...), custom_call_target="tpu_custom_call" | custom-call | tf_op jit(solution)/shard_map/pallas_call | solution.py:472
  30.5 1.1 %copy.15 = bf16[1,384,2048]{2,1,0:T(8,128)(2,1)} copy(bf16[1,384,2048]{2,1,0:T(8,128)(2,1)S(1)} %shard_map.127) | data formatting | bytes 3145728
